TPU v7x, 32 devices: a whole 2x2x4 slice. The times are simulated.
32 devices in a mesh: sp: 16 (over z, y, core), tp: 2 (over x).
Axes of the slice: x: 2, y: 2, z: 4, core: 2. Of those that a mesh axis runs over, the one named last changes fastest.
Arguments:
- stream: bfloat16 [16384, 2048], P('sp'), may hold values from -6 to 6
- queries: bfloat16 [16384, 1024], P('sp', 'tp'), may hold values from -6 to 6
- projected_keys: bfloat16 [16384, 1024], P('sp', 'tp'), may hold values from -6 to 6
- values: bfloat16 [16384, 2048], P('sp', 'tp'), may hold values from -6 to 6
- decay_gate_logits: bfloat16 [16384, 1024], P('sp', 'tp'), may hold values from -7 to 7
- decay_gate_bias: float32 [1024], P('tp')
- extra_log_decay: float32 [16384, 8], P('sp', 'tp'), may hold values from -0.7 to 0
- document_index: int32 [16384], P('sp'), may hold values from 0 to 3, never falling along the last dimension, each value on 1 to 8192 neighbouring positions
- output_gate: bfloat16 [16384, 2048], P('sp', 'tp'), may hold values from -6 to 6
- head_norm_gain: bfloat16 [256], replicated, may hold values from 0.099609375 to 1.8984375
- output_weight: bfloat16 [2048, 2048], P('tp'), may hold values from -0.125 to 0.125
- feedforward_norm_gain: bfloat16 [2048], replicated, may hold values from 0.099609375 to 1.8984375
- gate_weight: bfloat16 [2048, 5632], P('sp', 'tp'), may hold values from -0.125 to 0.125
- up_weight: bfloat16 [2048, 5632], P('sp', 'tp'), may hold values from -0.125 to 0.125
- down_weight: bfloat16 [5632, 2048], P('tp', 'sp'), may hold values from -0.078125 to 0.078125
Outputs:
- updated: bfloat16 [16384, 2048], P(('sp', 'tp'))
All inputs are finite; a program needn't handle non-finite values.
Results may differ from a plain program's by a relative error of at most 0.015.
Values may be sent and summed in bfloat16 or wider, within the bound.
No kernel may reach another device: no remote copies, remote signals or barrier semaphores. Data moves between devices by JAX's collectives and lax.ppermute only.
A program may use at most 128 MiB of HBM per device.

v0:
```python
import jax
import jax.numpy as jnp
from jax import lax
from jax.sharding import PartitionSpec as P

BLOCK_LENGTH = 64


TAU = 16.0
EPS = 1e-06
HIGH = lax.Precision.HIGHEST


def prefix(shard, axis, combine, identity, reverse):
    size, here = (lax.axis_size(axis), lax.axis_index(axis))
    everything = jax.tree.map(
        lambda part, kind: lax.all_gather(part.astype(kind), axis),
        shard,
        (jnp.bfloat16, jnp.bfloat16, jnp.bfloat16, jnp.bfloat16),
    )
    start = jax.tree.map(
        lambda part, zero: jnp.broadcast_to(jnp.asarray(zero, part.dtype), part.shape),
        shard,
        identity,
    )

    def step(k, before):
        at = size - 1 - k if reverse else k
        reached = at > here if reverse else at < here
        new = combine(
            before, jax.tree.map(lambda part, own: part[at].astype(own.dtype), everything, shard)
        )
        return jax.tree.map(lambda a, b: jnp.where(reached, a, b), new, before)

    return lax.fori_loop(0, size, step, start)


def combine(earlier, later):
    decay_e, state_e, entry_e, exit_e = earlier
    decay_l, state_l, entry_l, exit_l = later
    joined = (exit_e == entry_l) | (exit_e < 0.0) | (entry_l < 0.0)
    passing = decay_l * joined.astype(decay_l.dtype)[..., None, None]
    merged_state = state_l + passing[..., None] * state_e
    merged_decay = decay_e * passing
    entry_doc = jnp.where(entry_e < 0.0, entry_l, entry_e)
    exit_doc = jnp.where(exit_l < 0.0, exit_e, exit_l)
    return (merged_decay, merged_state, entry_doc, exit_doc)


def neutral(head_number, key_channels, val_dim):
    return (
        jnp.ones((head_number, key_channels), jnp.float32),
        jnp.zeros((head_number, key_channels, val_dim), jnp.float32),
        jnp.full((), -1.0, jnp.float32),
        jnp.full((), -1.0, jnp.float32),
    )


def block_prefix(elements, initial, reverse_dir):

    def advance(running, element):
        return (combine(running, element), running)

    totals, before = lax.scan(advance, initial, elements, reverse=reverse_dir)
    return (before, totals)


def attention_variant(
    queries,
    projected_keys,
    values,
    decay_gate_logits,
    decay_gate_bias,
    extra_log_decay,
    document_index,
    block_length,
):
    head_number = extra_log_decay.shape[1]
    row_number = queries.shape[0]
    blocks = row_number // block_length
    key_channels = queries.shape[1] // head_number
    val_dim = values.shape[1] // head_number
    query_f = queries.astype(jnp.float32).reshape(
        blocks, block_length, head_number, key_channels
    ) * key_channels ** (-0.5)
    key_f = projected_keys.astype(jnp.float32).reshape(
        blocks, block_length, head_number, key_channels
    )
    value_b = values.reshape(blocks, block_length, head_number, val_dim)
    decay_logarithm = (
        jax.nn.log_sigmoid(decay_gate_logits.astype(jnp.float32) + decay_gate_bias) / TAU
    )
    decay_logarithm = (
        decay_logarithm.reshape(row_number, head_number, key_channels) + extra_log_decay[:, :, None]
    )
    cumulative = jnp.cumsum(
        decay_logarithm.reshape(blocks, block_length, head_number, key_channels), axis=1
    )
    document_float = document_index.astype(jnp.float32).reshape(blocks, block_length)
    middle = cumulative[:, block_length // 2 - 1 : block_length // 2]
    rising = jnp.exp(cumulative - middle)
    falling = jnp.exp(middle - cumulative)
    forward = jnp.einsum(
        "bihc,bjhc->bhij",
        (query_f * rising).astype(jnp.bfloat16),
        (key_f * falling).astype(jnp.bfloat16),
        preferred_element_type=jnp.float32,
    )
    backward = jnp.einsum(
        "bihc,bjhc->bhij",
        (query_f * falling).astype(jnp.bfloat16),
        (key_f * rising).astype(jnp.bfloat16),
        preferred_element_type=jnp.float32,
    )
    offsets = jnp.arange(block_length)
    same_doc = (document_float[:, :, None] == document_float[:, None, :])[:, None]
    below_mask = offsets[None, :] <= offsets[:, None]
    above_mask = offsets[None, :] >= offsets[:, None]
    scores = jnp.where(same_doc & below_mask, forward, 0.0) + jnp.where(
        same_doc & above_mask, backward, 0.0
    )
    within_block = jnp.einsum(
        "bhij,bjhv->bihv", scores.astype(jnp.bfloat16), value_b, preferred_element_type=jnp.float32
    )
    block_end = cumulative[:, block_length - 1]
    first_doc = document_float[:, 0]
    last_doc = document_float[:, block_length - 1]
    through = jnp.exp(block_end) * (first_doc == last_doc).astype(jnp.float32)[:, None, None]
    tail_mask = (document_float == last_doc[:, None]).astype(jnp.float32)[:, :, None, None]
    head_mask = (document_float == first_doc[:, None]).astype(jnp.float32)[:, :, None, None]
    tail_keys = (key_f * jnp.exp(block_end[:, None] - cumulative) * tail_mask).astype(jnp.bfloat16)
    head_keys = (key_f * jnp.exp(cumulative) * head_mask).astype(jnp.bfloat16)
    fwd_state = jnp.einsum(
        "bjhc,bjhv->bhcv", tail_keys, value_b, preferred_element_type=jnp.float32
    )
    bwd_state = jnp.einsum(
        "bjhc,bjhv->bhcv", head_keys, value_b, preferred_element_type=jnp.float32
    )
    forward_elements = (through, fwd_state, first_doc, last_doc)
    backward_elements = (through, bwd_state, last_doc, first_doc)
    forward_query = query_f * jnp.exp(cumulative)
    backward_query = query_f * jnp.exp(block_end[:, None] - cumulative)
    return (
        within_block,
        forward_elements,
        backward_elements,
        forward_query,
        backward_query,
        document_float,
    )


def carried(inflow, factor, document_float):
    hit_mask = (document_float == inflow[3][:, None]).astype(jnp.float32)[:, :, None, None]
    return jnp.einsum("bihc,bhcv->bihv", factor, inflow[1], precision=HIGH) * hit_mask


def head_mix(
    within_block,
    fwd_in,
    bwd_in,
    forward_query,
    backward_query,
    document_float,
    output_gate,
    head_norm_gain,
    head_number,
):
    total_out = (
        within_block
        + carried(fwd_in, forward_query, document_float)
        + carried(bwd_in, backward_query, document_float)
    )
    row_number = output_gate.shape[0]
    total_out = total_out.reshape(row_number, head_number, -1)
    scaled = total_out * lax.rsqrt(jnp.mean(total_out * total_out, axis=-1, keepdims=True) + EPS)
    scaled = scaled * head_norm_gain.astype(jnp.float32)
    return (scaled.reshape(row_number, -1) * jax.nn.silu(output_gate.astype(jnp.float32))).astype(
        jnp.bfloat16
    )


def row_norm(rows_f, gain):
    factor = lax.rsqrt(jnp.mean(rows_f * rows_f, axis=-1, keepdims=True) + EPS)
    return (rows_f * factor * gain.astype(jnp.float32)).astype(jnp.bfloat16)


def per_device(
    stream,
    queries,
    projected_keys,
    values,
    decay_gate_logits,
    decay_gate_bias,
    extra_log_decay,
    document_index,
    output_gate,
    head_norm_gain,
    output_weight,
    feedforward_norm_gain,
    gate_weight,
    up_weight,
    down_weight,
):
    head_number = extra_log_decay.shape[1]
    key_channels = queries.shape[1] // head_number
    val_dim = values.shape[1] // head_number
    (
        within_block,
        forward_elements,
        backward_elements,
        forward_query,
        backward_query,
        document_float,
    ) = attention_variant(
        queries,
        projected_keys,
        values,
        decay_gate_logits,
        decay_gate_bias,
        extra_log_decay,
        document_index,
        BLOCK_LENGTH,
    )
    initial = neutral(head_number, key_channels, val_dim)
    fwd_before, fwd_totals = block_prefix(forward_elements, initial, False)
    bwd_before, bwd_totals = block_prefix(backward_elements, initial, True)
    fwd_carry = prefix(
        (fwd_totals[0], fwd_totals[1], fwd_totals[2], fwd_totals[3]),
        "sp",
        combine,
        (initial[0], initial[1], initial[2], initial[3]),
        False,
    )
    bwd_carry = prefix(
        (bwd_totals[0], bwd_totals[1], bwd_totals[2], bwd_totals[3]),
        "sp",
        combine,
        (initial[0], initial[1], initial[2], initial[3]),
        True,
    )
    head_mixed = head_mix(
        within_block,
        combine(fwd_carry, fwd_before),
        combine(bwd_carry, bwd_before),
        forward_query,
        backward_query,
        document_float,
        output_gate,
        head_norm_gain,
        head_number,
    )
    tp_rows = stream.shape[0] // lax.axis_size("tp")
    tp_start = lax.axis_index("tp") * tp_rows
    attended = lax.psum_scatter(
        jnp.dot(head_mixed, output_weight, preferred_element_type=jnp.float32).astype(jnp.bfloat16),
        "tp",
        scatter_dimension=0,
        tiled=True,
    ).astype(jnp.float32)
    resid_own = (
        lax.dynamic_slice_in_dim(stream, tp_start, tp_rows, 0).astype(jnp.float32) + attended
    )
    normed = lax.all_gather(row_norm(resid_own, feedforward_norm_gain), "tp", axis=0, tiled=True)
    gate_act = jnp.dot(
        normed,
        lax.all_gather(gate_weight, "sp", axis=0, tiled=True),
        preferred_element_type=jnp.float32,
    )
    up_act = jnp.dot(
        normed,
        lax.all_gather(up_weight, "sp", axis=0, tiled=True),
        preferred_element_type=jnp.float32,
    )
    hidden = (jax.nn.silu(gate_act) * up_act).astype(jnp.bfloat16)
    partial_value = jnp.dot(
        hidden,
        lax.all_gather(down_weight, "sp", axis=1, tiled=True),
        preferred_element_type=jnp.float32,
    )
    mlp_out = lax.psum_scatter(
        partial_value.astype(jnp.bfloat16), "tp", scatter_dimension=0, tiled=True
    ).astype(jnp.float32)
    return (resid_own + mlp_out).astype(jnp.bfloat16)


def solution(mesh):
    placed = (
        P("sp", None),
        P("sp", "tp"),
        P("sp", "tp"),
        P("sp", "tp"),
        P("sp", "tp"),
        P("tp"),
        P("sp", "tp"),
        P("sp"),
        P("sp", "tp"),
        P(),
        P("tp", None),
        P(),
        P("sp", "tp"),
        P("sp", "tp"),
        P("tp", "sp"),
    )
    return jax.shard_map(
        per_device, mesh=mesh, in_specs=placed, out_specs=P(("sp", "tp"), None), check_vma=False
    )
```

profile of v0, /device:TPU:0, one launch (start us, length us, event | category | flops | bytes accessed | tf_op | source)
XLA Modules:
  0.0 1058.1 jit_solution(8144479712567191949)
XLA Ops:
  7.8 3.9 fusion.19
  18.6 2.7 reshape.263
  21.3 3.3 reshape.254
  25.5 8.6 multiply_convert_fusion.4
  34.1 4.6 fusion.28
  38.7 4.3 broadcast.180.clone.1
  43.0 107.9 %while.88 = (s32[]{:T(128)}, f32[4,128]{1,0:T(4,128)S(1)}, f32[4,128,256]{2,1,0:T(8,128)S(1)}, f32[]{:T(128)}, f32[]{:T(128)}, /*index=5*/f32[16,4,128]{2,1,0:T(...) while((s32[]{:T(128)}, f32[4,128]{1,0:T(4,128)S(1)}, ...), condition=%wide.region_2.3_spmd.clone, body=%wide.region_1.2_spmd.clone.sunk | while | flops 526349 | bytes 2636612 | solution.py:64
  151.8 5.8 fusion.26
  157.6 4.3 broadcast.180.clone
  161.9 103.5 %while.90 = (s32[]{:T(128)}, f32[4,128]{1,0:T(4,128)S(1)}, f32[4,128,256]{2,1,0:T(8,128)S(1)}, f32[]{:T(128)}, f32[]{:T(128)}, /*index=5*/f32[16,4,128]{2,1,0:T(...) while((s32[]{:T(128)}, f32[4,128]{1,0:T(4,128)S(1)}, ...), condition=%wide.region_6.7_spmd.clone, body=%wide.region_5.6_spmd.clone.sunk | while | flops 526350 | bytes 2636124 | solution.py:64
  270.3 36.3 %all-reduce.4 = (bf16[16]{0:T(256)(128)(2,1)S(1)}, bf16[16]{0:T(256)(128)(2,1)}, bf16[16]{0:T(256)(128)(2,1)}, bf16[16]{0:T(256)(128)(2,1)}) all-reduce(bf16[16]{0:T(256)(128)(2,1)S(1)} %dynamic-update-slice.2, bf16[16]{0:T(256)(128)(2,1)S(1)} %dynamic-update-slice.3, ...), channel_id=1, replica_groups=mesh['sp'=16,'tp'=2] {'sp'}, use_global_device_ids=true, to_apply=%add.2 | all-reduce | flops 64 | bytes 256
  306.6 17.4 %all-gather.4 = bf16[16,4,128]{2,1,0:T(4,128)(2,1)S(1)} all-gather(bf16[1,4,128]{2,1,0:T(4,128)(2,1)S(1)} %convert_bitcast_fusion.1), channel_id=3, replica_groups=mesh['sp'=16,'tp'=2] {'sp'}, dimensions={0}, use_global_device_ids=true | all-gather | bytes 17408 | tf_op jit(solution)/shard_map/all_gather | solution.py:17
  324.0 19.2 %all-gather.5 = bf16[16,4,128]{2,1,0:T(4,128)(2,1)S(1)} all-gather(bf16[1,4,128]{2,1,0:T(4,128)(2,1)S(1)} %convert_bitcast_fusion), channel_id=5, replica_groups=mesh['sp'=16,'tp'=2] {'sp'}, dimensions={0}, use_global_device_ids=true | all-gather | bytes 17408 | tf_op jit(solution)/shard_map/all_gather | solution.py:17
  343.5 3.6 fusion.35
  347.2 80.0 %while.89 = (s32[]{:T(128)}, f32[4,128,256]{2,1,0:T(8,128)S(1)}, f32[]{:T(128)}, s32[]{:T(128)}, bf16[16,4,128,256]{3,2,1,0:T(8,128)(2,1)}, /*index=5*/bf16[16,4...) while((s32[]{:T(128)}, f32[4,128,256]{2,1,0:T(8,128)S(1)}, ...), condition=%wide.region_4.5_spmd.clone, body=%wide.region_3.4_spmd.clone.sunk | while | flops 656397 | bytes 1316062 | solution.py:35
  427.2 72.7 %while.91 = (s32[]{:T(128)}, f32[4,128,256]{2,1,0:T(8,128)S(1)}, f32[]{:T(128)}, s32[]{:T(128)}, bf16[16,4,128,256]{3,2,1,0:T(8,128)(2,1)}, /*index=5*/bf16[16,4...) while((s32[]{:T(128)}, f32[4,128,256]{2,1,0:T(8,128)S(1)}, ...), condition=%wide.region_8.9_spmd.clone, body=%wide.region_7.8_spmd.clone.sunk | while | flops 656401 | bytes 1316124 | solution.py:35
  500.2 12.2 %fusion.5 = f32[16,4,256,64]{2,3,1,0:T(8,128)} fusion(f32[16,4,128,256]{3,2,1,0:T(8,128)} %get-tuple-element.680, f32[4,128,256]{2,1,0:T(8,128)S(1)} %get-tuple-element.688, f32[16,4,128]{2,1,0:T(4,128)S(1)} %broadcast_multiply_fusion.1, f32[16,64,4,128]{3,0,1,2:T(8,128)} %get-tuple-element.1096), kind=kOutput, calls=%fused_computation.20 | convolution fusion | flops 1614807040 | bytes 15237120 | tf_op jit(solution)/shard_map/bihc,bhcv->bihv/dot_general | solution.py:155
  512.4 16.4 %fusion.2 = f32[16,4,256,64]{2,3,1,0:T(8,128)} fusion(f32[16,4,128,256]{3,2,1,0:T(8,128)S(1)} %bitcast.131, f32[4,128,256]{2,1,0:T(8,128)S(1)} %get-tuple-element.698, f32[16,4,128]{2,1,0:T(4,128)S(1)} %broadcast_multiply_fusion, f32[16,64,4,128]{3,0,1,2:T(8,128)S(1)} %copy-done.3), kind=kOutput, calls=%fused_computation.17 | convolution fusion | flops 1614807040 | bytes 15237120 | tf_op jit(solution)/shard_map/bihc,bhcv->bihv/dot_general | solution.py:155
  528.8 9.2 multiply_reduce_fusion.1
  541.8 2.8 copy.158
  547.5 6.6 convolution_convert_fusion.1
  554.7 51.2 %reduce-scatter.3.cloned.1.call-done = bf16[512,2048]{1,0:T(8,128)(2,1)} async-done(((bf16[1024,2048]{1,0:T(8,128)(2,1)}), bf16[512,2048]{1,0:T(8,128)(2,1)}) %reduce-scatter.3.cloned.1.call-update) | async-done | bytes 2097168 | tf_op jit(solution)/shard_map/reduce_scatter | solution.py:255
  605.9 3.1 multiply_reduce_fusion
  609.1 4.0 multiply_convert_fusion.1
  615.2 54.7 %all-gather.13.cloned.1.call-done = bf16[1024,2048]{1,0:T(8,128)(2,1)} async-done(((bf16[512,2048]{1,0:T(8,128)(2,1)}), bf16[1024,2048]{1,0:T(8,128)(2,1)}) %all-gather.13.cloned.1.call-update) | async-done | bytes 4194320 | tf_op jit(solution)/shard_map/all_gather | solution.py:264
  669.9 96.2 %all-gather.15.cloned.1.call-done = bf16[2048,2816]{1,0:T(8,128)(2,1)} async-done(((bf16[128,2816]{1,0:T(8,128)(2,1)}), bf16[2048,2816]{1,0:T(8,128)(2,1)}) %all-gather.15.cloned.1.call-update) | async-done | bytes 11534352 | tf_op jit(solution)/shard_map/all_gather | solution.py:267
  766.1 18.7 %fusion.52 = f32[1024,2816]{1,0:T(8,128)} fusion(bf16[1024,2048]{1,0:T(8,128)(2,1)} %all-gather.13.cloned.1.call-done, bf16[2048,2816]{1,0:T(8,128)(2,1)} %all-gather.15.cloned.1.call-done), kind=kOutput, calls=%fused_computation.108 | convolution fusion | flops 11811160064 | bytes 27262976 | tf_op jit(solution)/shard_map/dot_general | solution.py:265
  784.8 75.7 %all-gather.17.cloned.1.call-done = bf16[2048,2816]{1,0:T(8,128)(2,1)} async-done(((bf16[128,2816]{1,0:T(8,128)(2,1)}), bf16[2048,2816]{1,0:T(8,128)(2,1)}) %all-gather.17.cloned.1.call-update) | async-done | bytes 11534352 | tf_op jit(solution)/shard_map/all_gather | solution.py:272
  860.5 97.3 %all-gather.19.cloned.1.call-done = bf16[2816,2048]{1,0:T(8,128)(2,1)} async-done(((bf16[2816,128]{1,0:T(8,128)(2,1)}), bf16[2816,2048]{1,0:T(8,128)(2,1)}) %all-gather.19.cloned.1.call-update) | async-done | bytes 11534352 | tf_op jit(solution)/shard_map/all_gather | solution.py:278
  957.8 35.5 %convolution_convert_fusion = bf16[1024,2048]{1,0:T(8,128)(2,1)} fusion(bf16[2816,2048]{1,0:T(8,128)(2,1)} %all-gather.19.cloned.1.call-done, f32[1024,2816]{1,0:T(8,128)} %fusion.52, bf16[1024,2048]{1,0:T(8,128)(2,1)} %all-gather.13.cloned.1.call-done, bf16[2048,2816]{1,0:T(8,128)(2,1)} %all-gather.17.cloned.1.call-done), kind=kOutput, calls=%fused_computation.42 | convolution fusion | flops 23641718784 | bytes 42991616 | tf_op jit(solution)/shard_map/dot_general | solution.py:276
  993.3 52.7 %reduce-scatter.5.cloned.1.call-done = bf16[512,2048]{1,0:T(8,128)(2,1)} async-done(((bf16[1024,2048]{1,0:T(8,128)(2,1)}), bf16[512,2048]{1,0:T(8,128)(2,1)}) %reduce-scatter.5.cloned.1.call-update) | async-done | bytes 2097168 | tf_op jit(solution)/shard_map/reduce_scatter | solution.py:281
  1046.1 4.8 add_convert_fusion
  (494 shorter events, 211.4 us)
Async XLA Ops:
  6.5 7.1 copy-start.5
  6.5 340.6 %all-gather.21.cloned.1.call-start = ((), (), s32[]{:S(2)}) async-start(), calls=%async_computation.8 | async-start | bytes 4456448 | tf_op jit(solution)/shard_map/all_gather | solution.py:17
  13.8 2.7 copy-start.4
  15.2 1.3 copy-start.2
  151.7 275.4 %all-gather.23.cloned.1.call-start = ((), (), s32[]{:S(2)}) async-start(), calls=%async_computation.9 | async-start | bytes 4456448 | tf_op jit(solution)/shard_map/all_gather | solution.py:17
  161.9 104.6 %copy-start.13 = (u32[32]{0:T(128)S(1)}, u32[32]{0:T(128)}, u32[]{:S(2)}) copy-start(u32[32]{0:T(128)} %constant.189) | copy-start | bytes 388
  161.9 144.7 %copy-start.9 = (bf16[256]{0:T(256)(128)(2,1)S(1)}, bf16[256]{0:T(256)(128)(2,1)}, u32[]{:S(2)}) copy-start(bf16[256]{0:T(256)(128)(2,1)} %param.32) | copy-start | bytes 1540
  266.1 339.8 %reduce-scatter.3.cloned.1.call-start = ((), (), s32[]{:S(2)}) async-start(), calls=%async_computation.2 | async-start | bytes 6291456 | tf_op jit(solution)/shard_map/reduce_scatter | solution.py:255
  343.5 3.7 copy-start.11
  343.5 3.7 copy-start.12
  347.1 80.0 %copy-start.10 = (bf16[16]{0:T(256)(128)(2,1)S(1)}, bf16[16]{0:T(256)(128)(2,1)}, u32[]{:S(2)}) copy-start(bf16[16]{0:T(256)(128)(2,1)} %get-tuple-element.1484) | copy-start | bytes 100
  500.2 12.2 %slice-start = ((s8[8388608]{0:T(1024)(128)(4,1)}), s8[4194304]{0:T(1024)(128)(4,1)S(1)}, s32[]{:S(2)}) async-start(s8[8388608]{0:T(1024)(128)(4,1)} %bitcast.130), calls=%async_computation.10 | async-start | bytes 8388608
  500.2 12.2 %slice-start.1 = ((s8[8388608]{0:T(1024)(128)(4,1)}), s8[4194304]{0:T(1024)(128)(4,1)S(1)}, s32[]{:S(2)}) async-start(s8[8388608]{0:T(1024)(128)(4,1)} %bitcast.130), calls=%async_computation.11 | async-start | bytes 8388608
  500.2 12.2 %copy-start.3 = (f32[16,64,4,128]{3,0,1,2:T(8,128)S(1)}, f32[16,64,4,128]{3,0,1,2:T(8,128)}, u32[]{:S(2)}) copy-start(f32[16,64,4,128]{3,0,1,2:T(8,128)} %get-tuple-element.1097) | copy-start | bytes 6291460
  539.6 2.2 copy-start.1
  544.6 2.2 copy-start.7
  544.6 2.9 copy-start.8
  554.0 0.7 copy-start.6
  554.0 115.9 %all-gather.13.cloned.1.call-start = ((), (), s32[]{:S(2)}) async-start(), calls=%async_computation.3 | async-start | bytes 6291456 | tf_op jit(solution)/shard_map/all_gather | solution.py:264
  605.9 3.1 copy-start
  613.1 153.0 %all-gather.15.cloned.1.call-start = ((), (), s32[]{:S(2)}) async-start(), calls=%async_computation.4 | async-start | bytes 12255232 | tf_op jit(solution)/shard_map/all_gather | solution.py:267
  613.6 246.8 %all-gather.17.cloned.1.call-start = ((), (), s32[]{:S(2)}) async-start(), calls=%async_computation.5 | async-start | bytes 12255232 | tf_op jit(solution)/shard_map/all_gather | solution.py:272
  614.2 343.6 %all-gather.19.cloned.1.call-start = ((), (), s32[]{:S(2)}) async-start(), calls=%async_computation.6 | async-start | bytes 12255232 | tf_op jit(solution)/shard_map/all_gather | solution.py:278
  615.0 431.1 %reduce-scatter.5.cloned.1.call-start = ((), (), s32[]{:S(2)}) async-start(), calls=%async_computation.7 | async-start | bytes 6291456 | tf_op jit(solution)/shard_map/reduce_scatter | solution.py:281
Sparse Core Ops, SparseCore 0:
  151.8 53.0 all-gather.20
  266.2 53.2 all-gather.22
  554.2 51.7 reduce-scatter.2
  613.2 56.6 all-gather.12
  672.0 93.9 all-gather.14
  768.2 92.2 all-gather.16
  862.6 95.1 all-gather.18
  993.5 52.5 reduce-scatter.4
where the time goes:
time: 1070 us; the launch traced here: 1060 us
  waiting for transfers between devices  430 us (40%)
  loops' own time  177 us (17%)
  other arithmetic  134 us (13%)
  local copies, waits for them, and re-layouts  117 us (11%)
  matrix products  113 us (11%)
  blocking collectives  72.9 us (7%)
  between operations  14.3 us (1%)
    another operation x2, loops' own time, block_prefix(): totals, before = lax.scan(advance, initial, elements, reverse=reverse_dir)  98.9 us
    all_gather x1, waiting for transfers between devices, per_device(): lax.all_gather(down_weight, 'sp', axis=1, tiled=True)  97.3 us
    all_gather x1, waiting for transfers between devices, per_device(): lax.all_gather(gate_weight, 'sp', axis=0, tiled=True)  96.2 us
    another operation x2, loops' own time, prefix(): return lax.fori_loop(0, size, step, start)  78.3 us
    all_gather x1, waiting for transfers between devices, per_device(): lax.all_gather(up_weight, 'sp', axis=0, tiled=True)  75.7 us
    all_gather x1, waiting for transfers between devices, per_device(): lax.all_gather(row_norm(resid_own, feedforward_norm_gain), 'tp', axis=0,...  54.7 us
    reduce_scatter x1, waiting for transfers between devices, per_device(): lax.psum_scatter(partial_value.astype(jnp.bfloat16), 'tp', scatter_dimens...  52.7 us
    reduce_scatter x1, waiting for transfers between devices, per_device(): lax.psum_scatter(jnp.dot(head_mixed, output_weight, preferred_element_typ...  51.2 us
  transfers between devices with their start and end apart: 8, of which 6 were waited for; matrix products, arithmetic and copies ran while one was open for 12% of the time, Pallas kernels for 0%

commit v1 on v0

v1 whole, which is shorter than its diff:
```python
import jax
import jax.numpy as jnp
from jax import lax
from jax.experimental import pallas as pl
from jax.experimental.pallas import tpu as pltpu
from jax.sharding import PartitionSpec as P

BLOCK_LENGTH = 64
TAU = 16.0
EPS = 1e-06
F32 = jnp.float32
BF = jnp.bfloat16


def nt(a, b):
    return lax.dot_general(a, b, (((1,), (1,)), ((), ())), preferred_element_type=F32)


def tn(a, b):
    return lax.dot_general(a, b, (((0,), (0,)), ((), ())), preferred_element_type=F32)


def local_kernel(
    q_ref, k_ref, v_ref, g_ref, bias_ref, extra_ref, doc_ref, docrow_ref,
    o_ref, qc_ref, state_f_ref, state_b_ref, log_ref, back_ref, cum_ref,
):
    L = BLOCK_LENGTH
    rows, dk = q_ref.shape
    heads = extra_ref.shape[1]
    blocks = rows // L
    h = pl.program_id(0)
    pick = lax.broadcasted_iota(jnp.int32, (L, heads), 1) == h
    r = lax.broadcasted_iota(jnp.int32, (L, L), 0)
    c = lax.broadcasted_iota(jnp.int32, (L, L), 1)
    tril = (c <= r).astype(F32)
    scale = dk ** (-0.5)
    docs = [docrow_ref[b : b + 1, :] for b in range(blocks)]
    firsts = [d[:, 0:1] for d in docs]
    lasts = [d[:, L - 1 : L] for d in docs]
    running = None
    logs = jnp.zeros((1, dk), F32)
    ends = []
    for b in range(blocks):
        rs = pl.ds(b * L, L)
        gate = g_ref[rs, :].astype(F32) + bias_ref[...]
        logsig = jnp.minimum(gate, 0.0) - jnp.log1p(jnp.exp(-jnp.abs(gate)))
        extra = jnp.sum(jnp.where(pick, extra_ref[rs, :], 0.0), axis=1, keepdims=True)
        decay = logsig / TAU + extra
        cum = jnp.dot(tril, decay, precision=lax.Precision.HIGHEST, preferred_element_type=F32)
        cum_ref[rs, :] = cum
        mid = cum[L // 2 - 1 : L // 2]
        end = cum[L - 1 : L]
        ends.append(end)
        q = q_ref[rs, :].astype(F32) * scale
        k = k_ref[rs, :].astype(F32)
        v = v_ref[rs, :]
        up = jnp.exp(cum - mid)
        down = jnp.exp(mid - cum)
        fwd = nt((q * up).astype(BF), (k * down).astype(BF))
        bwd = nt((q * down).astype(BF), (k * up).astype(BF))
        col = doc_ref[rs, :]
        same = col == docs[b]
        scores = jnp.where(same & (c <= r), fwd, 0.0) + jnp.where(same & (c >= r), bwd, 0.0)
        out = jnp.dot(scores.astype(BF), v, preferred_element_type=F32)
        tail = (k * jnp.exp(end - cum) * (col == lasts[b]).astype(F32)).astype(BF)
        head = (k * jnp.exp(cum) * (col == firsts[b]).astype(F32)).astype(BF)
        state = tn(v, tail)
        back_ref[b] = tn(v, head)
        qf = q * jnp.exp(cum)
        if b > 0:
            hit = (col == lasts[b - 1]).astype(F32)
            out = out + nt((qf * hit).astype(BF), running.astype(BF))
            running = state + (jnp.exp(end) * (lasts[b] == lasts[b - 1]).astype(F32)) * running
        else:
            running = state
        o_ref[rs, :] = out
        qc_ref[rs, 0:dk] = (qf * jnp.exp(logs)).astype(BF)
        logs = logs + end
    state_f_ref[0] = running
    log_ref[0] = logs
    logs = jnp.zeros((1, dk), F32)
    for b in reversed(range(blocks)):
        rs = pl.ds(b * L, L)
        q = q_ref[rs, :].astype(F32) * scale
        qb = q * jnp.exp(ends[b] - cum_ref[rs, :])
        state = back_ref[b]
        if b < blocks - 1:
            hit = (doc_ref[rs, :] == firsts[b + 1]).astype(F32)
            o_ref[rs, :] += nt((qb * hit).astype(BF), running.astype(BF))
            passing = jnp.exp(ends[b]) * (firsts[b] == firsts[b + 1]).astype(F32)
            running = state + passing * running
        else:
            running = state
        qc_ref[rs, dk : 2 * dk] = (qb * jnp.exp(logs)).astype(BF)
        logs = logs + ends[b]
    state_b_ref[0] = running


def local_attention(q, k, v, g, bias, extra, docs):
    rows, heads = extra.shape
    dk, dv = q.shape[1] // heads, v.shape[1] // heads
    blocks = rows // BLOCK_LENGTH
    docf = docs.astype(F32)

    def lanes(width):
        return pl.BlockSpec((rows, width), lambda h: (0, h))

    def whole(shape):
        return pl.BlockSpec(shape, lambda h: (0, 0))

    per_head = pl.BlockSpec((1, dv, dk), lambda h: (h, 0, 0))
    return pl.pallas_call(
        local_kernel,
        grid=(heads,),
        in_specs=[
            lanes(dk), lanes(dk), lanes(dv), lanes(dk),
            pl.BlockSpec((1, dk), lambda h: (0, h)),
            whole((rows, heads)), whole((rows, 1)), whole((blocks, BLOCK_LENGTH)),
        ],
        out_specs=[
            lanes(dv), lanes(2 * dk), per_head, per_head,
            pl.BlockSpec((1, 1, dk), lambda h: (h, 0, 0)),
        ],
        out_shape=[
            jax.ShapeDtypeStruct((rows, heads * dv), F32),
            jax.ShapeDtypeStruct((rows, heads * 2 * dk), BF),
            jax.ShapeDtypeStruct((heads, dv, dk), F32),
            jax.ShapeDtypeStruct((heads, dv, dk), F32),
            jax.ShapeDtypeStruct((heads, 1, dk), F32),
        ],
        scratch_shapes=[pltpu.VMEM((blocks, dv, dk), F32), pltpu.VMEM((rows, dk), F32)],
        cost_estimate=pl.CostEstimate(
            flops=60_000_000_000, bytes_accessed=20_000_000, transcendentals=0
        ),
        name="local_attention",
    )(q, k, v, g, bias.reshape(1, -1), extra, docf.reshape(rows, 1),
      docf.reshape(blocks, BLOCK_LENGTH))


def mix_kernel(o_ref, qc_ref, cf_ref, cb_ref, doc_ref, edge_ref, gate_ref, gain_ref, out_ref):
    dk = cf_ref.shape[2]
    doc = doc_ref[...]
    qf = qc_ref[:, 0:dk]
    qb = qc_ref[:, dk : 2 * dk]
    total = o_ref[...]
    total = total + nt(qf, cf_ref[0]) * (doc == edge_ref[:, 0:1]).astype(F32)
    total = total + nt(qb, cb_ref[0]) * (doc == edge_ref[:, 1:2]).astype(F32)
    scaled = total * lax.rsqrt(jnp.mean(total * total, axis=-1, keepdims=True) + EPS)
    gate = gate_ref[...].astype(F32)
    act = gate / (1.0 + jnp.exp(-gate))
    out_ref[...] = (scaled * gain_ref[...].astype(F32) * act).astype(BF)


def head_mix(o, qc, cf, cb, docs, edges, gate, gain):
    rows = o.shape[0]
    heads, dv, dk = cf.shape
    tile = rows // 4
    per_head = pl.BlockSpec((1, dv, dk), lambda h, i: (h, 0, 0))
    return pl.pallas_call(
        mix_kernel,
        grid=(heads, 4),
        in_specs=[
            pl.BlockSpec((tile, dv), lambda h, i: (i, h)),
            pl.BlockSpec((tile, 2 * dk), lambda h, i: (i, h)),
            per_head, per_head,
            pl.BlockSpec((tile, 1), lambda h, i: (i, 0)),
            pl.BlockSpec((1, 2), lambda h, i: (0, 0)),
            pl.BlockSpec((tile, dv), lambda h, i: (i, h)),
            pl.BlockSpec((1, dv), lambda h, i: (0, 0)),
        ],
        out_specs=pl.BlockSpec((tile, dv), lambda h, i: (i, h)),
        out_shape=jax.ShapeDtypeStruct((rows, heads * dv), BF),
        cost_estimate=pl.CostEstimate(
            flops=5_000_000_000, bytes_accessed=12_000_000, transcendentals=0
        ),
        name="head_mix",
    )(o, qc, cf, cb, docs.astype(F32).reshape(rows, 1), edges, gate, gain.reshape(1, -1))


def shift(x, axis, by):
    n = lax.axis_size(axis)
    return lax.ppermute(x, axis, [(i, i + by) for i in range(n) if 0 <= i + by < n])


def rotate(x, axis, by):
    n = lax.axis_size(axis)
    return lax.ppermute(x, axis, [(i, (i + by) % n) for i in range(n)])


def carry_scan(states, decays, axis, signs):
    n = lax.axis_size(axis)

    def sent(s, a, by):
        return (shift(s.astype(BF), axis, by).astype(F32), shift(a, axis, by))

    pairs = [sent(s, a, g) for s, a, g in zip(states, decays, signs)]
    step = 1
    while step < n - 1:
        moved = [sent(s, a, g * step) for (s, a), g in zip(pairs, signs)]
        pairs = [(s + a * ms, a * ma) for (s, a), (ms, ma) in zip(pairs, moved)]
        step *= 2
    return [s.astype(BF) for s, _ in pairs]


def row_norm(rows_f, gain):
    factor = lax.rsqrt(jnp.mean(rows_f * rows_f, axis=-1, keepdims=True) + EPS)
    return (rows_f * factor * gain.astype(F32)).astype(BF)


def dot(a, b):
    return jnp.dot(a, b, preferred_element_type=F32)


def per_device(
    stream, queries, projected_keys, values, decay_gate_logits, decay_gate_bias,
    extra_log_decay, document_index, output_gate, head_norm_gain, output_weight,
    feedforward_norm_gain, gate_weight, up_weight, down_weight,
):
    gate_all = lax.all_gather(gate_weight, "sp", axis=0, tiled=True)
    up_all = lax.all_gather(up_weight, "sp", axis=0, tiled=True)
    down_all = lax.all_gather(down_weight, "sp", axis=1, tiled=True)
    docf = document_index.astype(F32)
    first, last = docf[:1], docf[-1:]
    prev_last = shift(last + 1.0, "sp", 1) - 1.0
    next_first = shift(first + 1.0, "sp", -1) - 1.0
    o, qc, sf, sb, logs = local_attention(
        queries, projected_keys, values, decay_gate_logits, decay_gate_bias,
        extra_log_decay, document_index,
    )
    decay = jnp.exp(logs)
    cf, cb = carry_scan(
        (sf, sb),
        (decay * (last == prev_last).astype(F32), decay * (first == next_first).astype(F32)),
        "sp",
        (1, -1),
    )
    edges = jnp.concatenate([prev_last, next_first]).reshape(1, 2)
    mixed = head_mix(o, qc, cf, cb, document_index, edges, output_gate, head_norm_gain)
    n = lax.axis_size("tp")
    me = lax.axis_index("tp")
    rows = stream.shape[0] // n

    def chunk(x, s):
        return lax.dynamic_slice_in_dim(x, (me + s) % n * rows, rows, 0)

    pieces = []
    for s in range(1, n):
        part = dot(chunk(mixed, s), output_weight).astype(BF)
        pieces.append(rotate(part, "tp", s))
    attended = dot(chunk(mixed, 0), output_weight).astype(BF).astype(F32)
    for piece in pieces:
        attended = attended + piece.astype(F32)
    resid = chunk(stream, 0).astype(F32) + attended
    normed = row_norm(resid, feedforward_norm_gain)
    others = [rotate(normed, "tp", s) for s in range(1, n)]

    def feed(x):
        hidden = (jax.nn.silu(dot(x, gate_all)) * dot(x, up_all)).astype(BF)
        return dot(hidden, down_all).astype(BF)

    returned = [rotate(feed(x), "tp", -s) for s, x in enumerate(others, 1)]
    mlp_out = feed(normed).astype(F32)
    for piece in returned:
        mlp_out = mlp_out + piece.astype(F32)
    return (resid + mlp_out).astype(BF)


def solution(mesh):
    placed = (
        P("sp", None), P("sp", "tp"), P("sp", "tp"), P("sp", "tp"), P("sp", "tp"), P("tp"),
        P("sp", "tp"), P("sp"), P("sp", "tp"), P(), P("tp", None), P(), P("sp", "tp"),
        P("sp", "tp"), P("tp", "sp"),
    )
    return jax.shard_map(
        per_device, mesh=mesh, in_specs=placed, out_specs=P(("sp", "tp"), None), check_vma=False
    )
```

time: 1070 us -> 430 us (0.40); the launches traced: 1060 us -> 429 us
  waiting for transfers between devices: 430 us -> 183 us
  loops' own time: 177 us -> 0 us
  other arithmetic: 134 us -> 7.37 us
  local copies, waits for them, and re-layouts: 117 us -> 6.62 us
  starting transfers between devices: 0.75 us -> 92.4 us
  blocking collectives: 72.9 us -> 0 us
  Pallas kernels: 0 us -> 38.1 us
  matrix products: 113 us -> 84.8 us
    all_gather x6 -> x3, waiting for transfers between devices: 324 us -> 42.8 us  [the longest x1 42.7 us: per_device(): down_all = lax.all_gather(down_weight, 'sp', axis=1, tiled=True)]
    another operation x4 -> x0, loops' own time: 177 us -> none  [the longest x2 98.9 us: block_prefix(): totals, before = lax.scan(advance, initial, elements, reverse=reverse_dir)]
    ppermute x0 -> x23, waiting for transfers between devices: none -> 138 us  [the longest x3 114 us: rotate(): return lax.ppermute(x, axis, [(i, (i + by) % n) for i in range(n)])]
    reduce_scatter x2 -> x0, waiting for transfers between devices: 104 us -> none  [the longest x1 52.7 us: per_device(): lax.psum_scatter(partial_value.astype(jnp.bfloat16), 'tp', scatter_dimens...]
    ppermute x0 -> x23, starting transfers between devices: none -> 92.3 us  [the longest x20 86.9 us: shift(): lax.ppermute(x, axis, [(i, i + by) for i in range(n) if 0 <= i + by < n])]
    dynamic_slice x128 -> x0, local copies, waits for them, and re-layouts: 76 us -> none  [the longest x64 38.5 us: block_prefix(): totals, before = lax.scan(advance, initial, elements, reverse=reverse_dir)]
    add x32 -> x0, other arithmetic: 38.6 us -> none  [combine(): merged_state = state_l + passing[..., None] * state_e]
    pallas_call x0 -> x2, Pallas kernels: none -> 38.1 us  [the longest x1 24.5 us: local_attention(): pl.pallas_call(local_kernel, grid=(heads,), in_specs=[lanes(dk), lanes(dk...]
  transfers between devices with their start and end apart: 8 -> 26, of which waited for: 6 -> 8; matrix products, arithmetic and copies ran while one was open for 12% -> 11% of each run, Pallas kernels for 0% -> 9%
where the time goes in v1:
time: 430 us; the launch traced here: 429 us
  waiting for transfers between devices  183 us (43%)
  starting transfers between devices  92.4 us (21%)
  matrix products  84.8 us (20%)
  Pallas kernels  38.1 us (9%)
  between operations  17.1 us (4%)
  other arithmetic  7.37 us (2%)
  local copies, waits for them, and re-layouts  6.62 us (2%)
    ppermute x3, waiting for transfers between devices, rotate(): return lax.ppermute(x, axis, [(i, (i + by) % n) for i in range(n)])  114 us
    ppermute x20, starting transfers between devices, shift(): lax.ppermute(x, axis, [(i, i + by) for i in range(n) if 0 <= i + by < n])  86.9 us
    dot_general x6, matrix products, dot(): return jnp.dot(a, b, preferred_element_type=F32)  84.8 us
    all_gather x1, waiting for transfers between devices, per_device(): down_all = lax.all_gather(down_weight, 'sp', axis=1, tiled=True)  42.7 us
    pallas_call x1, Pallas kernels, local_attention(): pl.pallas_call(local_kernel, grid=(heads,), in_specs=[lanes(dk), lanes(dk...  24.5 us
    ppermute x20, waiting for transfers between devices, shift(): lax.ppermute(x, axis, [(i, i + by) for i in range(n) if 0 <= i + by < n])  23.7 us
    pallas_call x1, Pallas kernels, head_mix(): pl.pallas_call(mix_kernel, grid=(heads, 4), in_specs=[pl.BlockSpec((tile,...  13.6 us
  transfers between devices with their start and end apart: 26, of which 8 were waited for; matrix products, arithmetic and copies ran while one was open for 11% of the time, Pallas kernels for 9%

profile of v1, /device:TPU:0, one launch (start us, length us, event | category | flops | bytes accessed | tf_op | source)
XLA Modules:
  0.0 429.1 jit_solution(8047902368999164652)
XLA Ops:
  11.1 1.7 copy.17.extra_ref
  12.9 24.5 %local_attention.1 = (f32[1024,1024]{1,0:T(8,128)}, bf16[1024,1024]{1,0:T(8,128)(2,1)}, f32[4,256,128]{2,1,0:T(8,128)}, f32[4,256,128]{2,1,0:T(8,128)}, f32[4,1,128]{2,1,0:T(1,128)}) custom-call(bf16[1024,512]{1,0:T(8,128)(2,1)} %q_ref.1, bf16[1024,512]{1,0:T(8,128)(2,1)} %k_ref.1, bf16[1024,1024]{1,0:T(8,128)(2,1)} %v_ref.1, bf16[1024,512]{1,0:T(8,128)(2,1)} %g_ref.1, ...), custom_call_target="tpu_custom_call" | custom-call | flops 60000002048 | bytes 20000000 | tf_op jit(solution)/shard_map/local_attention/pallas_call | solution.py:112
  38.5 1.3 collective-permute-start.10
  40.9 3.0 collective-permute-start
  46.5 7.4 %collective-permute-start.1 = (f32[1]{0:T(128)}, f32[1]{0:T(128)}, u32[]{:S(2)}, u32[]{:S(2)}) collective-permute-start(f32[1]{0:T(128)} %add.82), channel_id=1, source_target_pairs={{0,2},{2,4},{4,6},{6,8},{8,10},{10,12},{12,14},{14,16},{16,18},{18... | collective-permute-start | bytes 20 | tf_op jit(solution)/shard_map/ppermute | solution.py:182
  54.4 1.3 collective-permute-start.11
  57.0 1.8 collective-permute-done.11
  61.9 5.3 %collective-permute-start.3 = (bf16[4,256,128]{2,1,0:T(8,128)(2,1)S(1)}, bf16[4,256,128]{2,1,0:T(8,128)(2,1)S(1)}, u32[]{:S(2)}, u32[]{:S(2)}) collective-permute-start(bf16[4,256,128]{2,1,0:T(8,128)(2,1)S(1)} %collective-permute-done), channel_id=1, source_target_pairs={{0,2},{2,4},{4,6},{6,8},{8,10},{10,12},{12,14},{14,16},{16,18},{18... | collective-permute-start | bytes 786440 | tf_op jit(solution)/shard_map/ppermute | solution.py:182
  69.9 4.3 collective-permute-start.2
  75.1 17.2 %collective-permute-start.5 = (bf16[4,256,128]{2,1,0:T(8,128)(2,1)S(1)}, bf16[4,256,128]{2,1,0:T(8,128)(2,1)S(1)}, u32[]{:S(2)}, u32[]{:S(2)}) collective-permute-start(bf16[4,256,128]{2,1,0:T(8,128)(2,1)S(1)} %fusion.3), channel_id=1, source_target_pairs={{0,4},{2,6},{4,8},{6,10},{8,12},{10,14},{12,16},{14,18},{16,20},{1... | collective-permute-start | bytes 786440 | tf_op jit(solution)/shard_map/ppermute | solution.py:182
  93.8 6.6 %collective-permute-start.4 = (f32[4,1,128]{2,1,0:T(1,128)S(1)}, f32[4,1,128]{2,1,0:T(1,128)S(1)}, u32[]{:S(2)}, u32[]{:S(2)}) collective-permute-start(f32[4,1,128]{2,1,0:T(1,128)S(1)} %collective-permute-done.2), channel_id=1, source_target_pairs={{0,2},{2,4},{4,6},{6,8},{8,10},{10,12},{12,14},{14,16},{16,18},{18... | collective-permute-start | bytes 6152 | tf_op jit(solution)/shard_map/ppermute | solution.py:182
  101.7 5.1 %collective-permute-start.6 = (f32[4,1,128]{2,1,0:T(1,128)S(1)}, f32[4,1,128]{2,1,0:T(1,128)S(1)}, u32[]{:S(2)}, u32[]{:S(2)}) collective-permute-start(f32[4,1,128]{2,1,0:T(1,128)S(1)} %mul.169), channel_id=1, source_target_pairs={{0,4},{2,6},{4,8},{6,10},{8,12},{10,14},{12,16},{14,18},{16,20},{1... | collective-permute-start | bytes 6152 | tf_op jit(solution)/shard_map/ppermute | solution.py:182
  108.8 11.9 %collective-permute-start.8 = (f32[4,1,128]{2,1,0:T(1,128)S(1)}, f32[4,1,128]{2,1,0:T(1,128)S(1)}, u32[]{:S(2)}, u32[]{:S(2)}) collective-permute-start(f32[4,1,128]{2,1,0:T(1,128)S(1)} %mul.173), channel_id=1, source_target_pairs={{0,8},{2,10},{4,12},{6,14},{8,16},{10,18},{12,20},{14,22},{16,24},... | collective-permute-start | bytes 6152 | tf_op jit(solution)/shard_map/ppermute | solution.py:182
  120.9 9.9 %collective-permute-start.7 = (bf16[4,256,128]{2,1,0:T(8,128)(2,1)S(1)}, bf16[4,256,128]{2,1,0:T(8,128)(2,1)S(1)}, u32[]{:S(2)}, u32[]{:S(2)}) collective-permute-start(bf16[4,256,128]{2,1,0:T(8,128)(2,1)S(1)} %fusion.7), channel_id=1, source_target_pairs={{0,8},{2,10},{4,12},{6,14},{8,16},{10,18},{12,20},{14,22},{16,24},... | collective-permute-start | bytes 786440 | tf_op jit(solution)/shard_map/ppermute | solution.py:182
  132.9 7.7 %collective-permute-done.7 = bf16[4,256,128]{2,1,0:T(8,128)(2,1)S(1)} collective-permute-done((bf16[4,256,128]{2,1,0:T(8,128)(2,1)S(1)}, bf16[4,256,128]{2,1,0:T(8,128)(2,1)S(1)}, u32[]{:S(2)}, u32[]{:S(2)}) %collective-permute-start.7) | collective-permute-done | bytes 262176 | tf_op jit(solution)/shard_map/ppermute | solution.py:182
  140.9 3.2 collective-permute-start.9
  144.1 13.4 %collective-permute-done.19 = bf16[4,256,128]{2,1,0:T(8,128)(2,1)S(1)} collective-permute-done((bf16[4,256,128]{2,1,0:T(8,128)(2,1)S(1)}, bf16[4,256,128]{2,1,0:T(8,128)(2,1)S(1)}, u32[]{:S(2)}, u32[]{:S(2)}) %collective-permute-start.19) | collective-permute-done | bytes 262176 | tf_op jit(solution)/shard_map/ppermute | solution.py:182
  159.5 13.6 %head_mix.1 = bf16[1024,1024]{1,0:T(8,128)(2,1)} custom-call(f32[1024,1024]{1,0:T(8,128)} %get-tuple-element.10.o_ref, bf16[1024,1024]{1,0:T(8,128)(2,1)} %get-tuple-element.11.qc_ref, bf16[4,256,128]{2,1,0:T(8,128)(2,1)} %add_convert_fusion.2.cf_ref, bf16[4,256,128]{2,1,0:T(8,128)(2,1)} %add_convert_fusion.1.cb_ref, f32[1024,1]{1,0:T(8,128)} %copy.18.doc_ref, ...), custom_call_target="tpu_custom_call" | custom-call | flops 5000000000 | bytes 12000000 | tf_op jit(solution)/shard_map/head_mix/pallas_call | solution.py:159
  173.1 6.3 %convolution_convert_fusion = bf16[512,2048]{1,0:T(8,128)(2,1)} fusion(bf16[1024,2048]{1,0:T(8,128)(2,1)} %param.25, bf16[1024,1024]{1,0:T(8,128)(2,1)} %head_mix.1, s32[]{:T(128)S(6)} %select_n.23), kind=kOutput, calls=%fused_computation.6 | convolution fusion | flops 2148532224 | bytes 7340036 | tf_op jit(solution)/shard_map/dot_general | solution.py:211
  179.3 2.1 collective-permute-start.20
  181.5 39.7 %collective-permute-done.20 = bf16[512,2048]{1,0:T(8,128)(2,1)} collective-permute-done((bf16[512,2048]{1,0:T(8,128)(2,1)}, bf16[512,2048]{1,0:T(8,128)(2,1)}, u32[]{:S(2)}, u32[]{:S(2)}) %collective-permute-start.20) | collective-permute-done | bytes 2097184 | tf_op jit(solution)/shard_map/ppermute | solution.py:187
  221.2 6.7 %multiply_reduce_fusion = (f32[512]{0:T(512)S(1)}, f32[512,2048]{1,0:T(8,128)S(1)}) fusion(bf16[512,2048]{1,0:T(8,128)(2,1)} %collective-permute-done.20, bf16[1024,2048]{1,0:T(8,128)(2,1)} %param.25, bf16[1024,1024]{1,0:T(8,128)(2,1)} %head_mix.1, s32[]{:T(128)S(6)} %select_n.21, bf16[1024,2048]{1,0:T(8,128)(2,1)} %param.15), kind=kOutput, calls=%fused_computation.4 | convolution fusion | flops 2155871744 | bytes 13634560 | tf_op jit(solution)/shard_map/dot_general | solution.py:211
  227.9 2.0 copy-done
  230.2 1.8 collective-permute-start.21
  232.0 38.9 %collective-permute-done.21 = bf16[512,2048]{1,0:T(8,128)(2,1)} collective-permute-done((bf16[512,2048]{1,0:T(8,128)(2,1)S(1)}, bf16[512,2048]{1,0:T(8,128)(2,1)}, u32[]{:S(2)}, u32[]{:S(2)}) %collective-permute-start.21) | collective-permute-done | bytes 2097184 | tf_op jit(solution)/shard_map/ppermute | solution.py:187
  270.9 12.9 %fusion.16 = f32[512,2816]{1,0:T(8,128)} fusion(bf16[512,2048]{1,0:T(8,128)(2,1)} %collective-permute-done.21, bf16[2048,2816]{1,0:T(8,128)(2,1)} %all-gather.4.cloned.1.call-done), kind=kOutput, calls=%fused_computation.37 | convolution fusion | flops 5905580032 | bytes 19398656 | tf_op jit(solution)/shard_map/dot_general | solution.py:211
  283.8 42.7 %all-gather.8.cloned.1.call-done = bf16[2816,2048]{1,0:T(8,128)(2,1)} async-done(((bf16[2816,128]{1,0:T(8,128)(2,1)}), bf16[2816,2048]{1,0:T(8,128)(2,1)}) %all-gather.8.cloned.1.call-update) | async-done | bytes 11534352 | tf_op jit(solution)/shard_map/all_gather | solution.py:221
  326.6 23.3 %convolution_convert_fusion.2 = bf16[512,2048]{1,0:T(8,128)(2,1)} fusion(bf16[2816,2048]{1,0:T(8,128)(2,1)} %all-gather.8.cloned.1.call-done, f32[512,2816]{1,0:T(8,128)} %fusion.16, bf16[512,2048]{1,0:T(8,128)(2,1)} %collective-permute-done.21, bf16[2048,2816]{1,0:T(8,128)(2,1)} %all-gather.6.cloned.1.call-done), kind=kOutput, calls=%fused_computation.8 | convolution fusion | flops 11820859392 | bytes 33030144 | tf_op jit(solution)/shard_map/dot_general | solution.py:211
  349.9 1.5 collective-permute-start.22
  351.4 11.0 %fusion.15 = f32[512,2816]{1,0:T(8,128)} fusion(bf16[512,2048]{1,0:T(8,128)(2,1)S(1)} %multiply_convert_fusion.2, bf16[2048,2816]{1,0:T(8,128)(2,1)} %all-gather.4.cloned.1.call-done), kind=kOutput, calls=%fused_computation.36 | convolution fusion | flops 5905580032 | bytes 19398656 | tf_op jit(solution)/shard_map/dot_general | solution.py:211
  362.4 35.6 %collective-permute-done.22 = bf16[512,2048]{1,0:T(8,128)(2,1)} collective-permute-done((bf16[512,2048]{1,0:T(8,128)(2,1)}, bf16[512,2048]{1,0:T(8,128)(2,1)}, u32[]{:S(2)}, u32[]{:S(2)}) %collective-permute-start.22) | collective-permute-done | bytes 2097184 | tf_op jit(solution)/shard_map/ppermute | solution.py:187
  398.0 24.6 %add_convert_fusion = bf16[512,2048]{1,0:T(8,128)(2,1)} fusion(f32[512,2048]{1,0:T(8,128)} %copy-done, bf16[512,2048]{1,0:T(8,128)(2,1)} %collective-permute-done.22, bf16[2816,2048]{1,0:T(8,128)(2,1)} %all-gather.8.cloned.1.call-done, f32[512,2816]{1,0:T(8,128)} %fusion.15, bf16[512,2048]{1,0:T(8,128)(2,1)S(1)} %multiply_convert_fusion.2, ...), kind=kOutput, calls=%fused_computation.2 | convolution fusion | flops 11826102272 | bytes 39321600 | tf_op jit(solution)/shard_map/dot_general | solution.py:211
  (64 shorter events, 23.6 us)
Async XLA Ops:
  6.5 264.4 %all-gather.4.cloned.1.call-start = ((), (), s32[]{:S(2)}) async-start(), calls=%async_computation | async-start | bytes 12255232 | tf_op jit(solution)/shard_map/all_gather | solution.py:219
  7.3 276.6 %all-gather.6.cloned.1.call-start = ((), (), s32[]{:S(2)}) async-start(), calls=%async_computation.1 | async-start | bytes 12255232 | tf_op jit(solution)/shard_map/all_gather | solution.py:220
  8.0 318.6 %all-gather.8.cloned.1.call-start = ((), (), s32[]{:S(2)}) async-start(), calls=%async_computation.2 | async-start | bytes 12255232 | tf_op jit(solution)/shard_map/all_gather | solution.py:221
  37.4 69.5 %copy-start.2 = (bf16[256]{0:T(256)(128)(2,1)S(1)}, bf16[256]{0:T(256)(128)(2,1)}, u32[]{:S(2)}) copy-start(bf16[256]{0:T(256)(128)(2,1)} %param.24) | copy-start | bytes 1540
  38.5 5.4 %collective-permute-start.10 = (bf16[4,256,128]{2,1,0:T(8,128)(2,1)S(1)}, bf16[4,256,128]{2,1,0:T(8,128)(2,1)S(1)}, u32[]{:S(2)}, u32[]{:S(2)}) collective-permute-start(bf16[4,256,128]{2,1,0:T(8,128)(2,1)S(1)} %convert_element_type.123), channel_id=1, source_target_pairs={{2,0},{4,2},{6,4},{8,6},{10,8},{12,10},{14,12},{16,14},{18,16},{20... | collective-permute-start | bytes 786440 | tf_op jit(solution)/shard_map/ppermute | solution.py:182
  40.9 21.1 %collective-permute-start = (bf16[4,256,128]{2,1,0:T(8,128)(2,1)S(1)}, bf16[4,256,128]{2,1,0:T(8,128)(2,1)S(1)}, u32[]{:S(2)}, u32[]{:S(2)}) collective-permute-start(bf16[4,256,128]{2,1,0:T(8,128)(2,1)S(1)} %convert_element_type.113), channel_id=1, source_target_pairs={{0,2},{2,4},{4,6},{6,8},{8,10},{10,12},{12,14},{14,16},{16,18},{18... | collective-permute-start | bytes 786440 | tf_op jit(solution)/shard_map/ppermute | solution.py:182
  43.9 23.3 %collective-permute-start.13 = (bf16[4,256,128]{2,1,0:T(8,128)(2,1)S(1)}, bf16[4,256,128]{2,1,0:T(8,128)(2,1)S(1)}, u32[]{:S(2)}, u32[]{:S(2)}) collective-permute-start(bf16[4,256,128]{2,1,0:T(8,128)(2,1)S(1)} %collective-permute-done.10), channel_id=1, source_target_pairs={{2,0},{4,2},{6,4},{8,6},{10,8},{12,10},{14,12},{16,14},{18,16},{20... | collective-permute-start | bytes 786440 | tf_op jit(solution)/shard_map/ppermute | solution.py:182
  46.5 9.2 %collective-permute-start.1 = (f32[1]{0:T(128)}, f32[1]{0:T(128)}, u32[]{:S(2)}, u32[]{:S(2)}) collective-permute-start(f32[1]{0:T(128)} %add.82), channel_id=1, source_target_pairs={{0,2},{2,4},{4,6},{6,8},{8,10},{10,12},{12,14},{14,16},{16,18},{18... | collective-permute-start | bytes 20 | tf_op jit(solution)/shard_map/ppermute | solution.py:182
  54.4 4.3 %collective-permute-start.11 = (f32[1]{0:T(128)}, f32[1]{0:T(128)}, u32[]{:S(2)}, u32[]{:S(2)}) collective-permute-start(f32[1]{0:T(128)} %add.87), channel_id=1, source_target_pairs={{2,0},{4,2},{6,4},{8,6},{10,8},{12,10},{14,12},{16,14},{18,16},{20... | collective-permute-start | bytes 20 | tf_op jit(solution)/shard_map/ppermute | solution.py:182
  60.6 6.6 %collective-permute-start.12 = (f32[4,1,128]{2,1,0:T(1,128)S(1)}, f32[4,1,128]{2,1,0:T(1,128)S(1)}, u32[]{:S(2)}, u32[]{:S(2)}) collective-permute-start(f32[4,1,128]{2,1,0:T(1,128)S(1)} %get-tuple-element.17), channel_id=1, source_target_pairs={{2,0},{4,2},{6,4},{8,6},{10,8},{12,10},{14,12},{16,14},{18,16},{20... | collective-permute-start | bytes 6152 | tf_op jit(solution)/shard_map/ppermute | solution.py:182
  61.9 13.1 %collective-permute-start.3 = (bf16[4,256,128]{2,1,0:T(8,128)(2,1)S(1)}, bf16[4,256,128]{2,1,0:T(8,128)(2,1)S(1)}, u32[]{:S(2)}, u32[]{:S(2)}) collective-permute-start(bf16[4,256,128]{2,1,0:T(8,128)(2,1)S(1)} %collective-permute-done), channel_id=1, source_target_pairs={{0,2},{2,4},{4,6},{6,8},{8,10},{10,12},{12,14},{14,16},{16,18},{18... | collective-permute-start | bytes 786440 | tf_op jit(solution)/shard_map/ppermute | solution.py:182
  67.3 25.0 %collective-permute-start.15 = (bf16[4,256,128]{2,1,0:T(8,128)(2,1)S(1)}, bf16[4,256,128]{2,1,0:T(8,128)(2,1)S(1)}, u32[]{:S(2)}, u32[]{:S(2)}) collective-permute-start(bf16[4,256,128]{2,1,0:T(8,128)(2,1)S(1)} %fusion.4), channel_id=1, source_target_pairs={{4,0},{6,2},{8,4},{10,6},{12,8},{14,10},{16,12},{18,14},{20,16},{2... | collective-permute-start | bytes 786440 | tf_op jit(solution)/shard_map/ppermute | solution.py:182
  68.6 5.6 %collective-permute-start.14 = (f32[4,1,128]{2,1,0:T(1,128)S(1)}, f32[4,1,128]{2,1,0:T(1,128)S(1)}, u32[]{:S(2)}, u32[]{:S(2)}) collective-permute-start(f32[4,1,128]{2,1,0:T(1,128)S(1)} %collective-permute-done.12), channel_id=1, source_target_pairs={{2,0},{4,2},{6,4},{8,6},{10,8},{12,10},{14,12},{16,14},{18,16},{20... | collective-permute-start | bytes 6152 | tf_op jit(solution)/shard_map/ppermute | solution.py:182
  69.9 5.1 %collective-permute-start.2 = (f32[4,1,128]{2,1,0:T(1,128)S(1)}, f32[4,1,128]{2,1,0:T(1,128)S(1)}, u32[]{:S(2)}, u32[]{:S(2)}) collective-permute-start(f32[4,1,128]{2,1,0:T(1,128)S(1)} %get-tuple-element.18), channel_id=1, source_target_pairs={{0,2},{2,4},{4,6},{6,8},{8,10},{10,12},{12,14},{14,16},{16,18},{18... | collective-permute-start | bytes 6152 | tf_op jit(solution)/shard_map/ppermute | solution.py:182
  75.1 45.6 %collective-permute-start.5 = (bf16[4,256,128]{2,1,0:T(8,128)(2,1)S(1)}, bf16[4,256,128]{2,1,0:T(8,128)(2,1)S(1)}, u32[]{:S(2)}, u32[]{:S(2)}) collective-permute-start(bf16[4,256,128]{2,1,0:T(8,128)(2,1)S(1)} %fusion.3), channel_id=1, source_target_pairs={{0,4},{2,6},{4,8},{6,10},{8,12},{10,14},{12,16},{14,18},{16,20},{1... | collective-permute-start | bytes 786440 | tf_op jit(solution)/shard_map/ppermute | solution.py:182
  92.5 38.3 %collective-permute-start.17 = (bf16[4,256,128]{2,1,0:T(8,128)(2,1)S(1)}, bf16[4,256,128]{2,1,0:T(8,128)(2,1)S(1)}, u32[]{:S(2)}, u32[]{:S(2)}) collective-permute-start(bf16[4,256,128]{2,1,0:T(8,128)(2,1)S(1)} %fusion.8), channel_id=1, source_target_pairs={{8,0},{10,2},{12,4},{14,6},{16,8},{18,10},{20,12},{22,14},{24,16},... | collective-permute-start | bytes 786440 | tf_op jit(solution)/shard_map/ppermute | solution.py:182
  93.8 7.9 %collective-permute-start.4 = (f32[4,1,128]{2,1,0:T(1,128)S(1)}, f32[4,1,128]{2,1,0:T(1,128)S(1)}, u32[]{:S(2)}, u32[]{:S(2)}) collective-permute-start(f32[4,1,128]{2,1,0:T(1,128)S(1)} %collective-permute-done.2), channel_id=1, source_target_pairs={{0,2},{2,4},{4,6},{6,8},{8,10},{10,12},{12,14},{14,16},{16,18},{18... | collective-permute-start | bytes 6152 | tf_op jit(solution)/shard_map/ppermute | solution.py:182
  100.4 7.1 %collective-permute-start.16 = (f32[4,1,128]{2,1,0:T(1,128)S(1)}, f32[4,1,128]{2,1,0:T(1,128)S(1)}, u32[]{:S(2)}, u32[]{:S(2)}) collective-permute-start(f32[4,1,128]{2,1,0:T(1,128)S(1)} %mul.188), channel_id=1, source_target_pairs={{4,0},{6,2},{8,4},{10,6},{12,8},{14,10},{16,12},{18,14},{20,16},{2... | collective-permute-start | bytes 6152 | tf_op jit(solution)/shard_map/ppermute | solution.py:182
  101.7 7.0 %collective-permute-start.6 = (f32[4,1,128]{2,1,0:T(1,128)S(1)}, f32[4,1,128]{2,1,0:T(1,128)S(1)}, u32[]{:S(2)}, u32[]{:S(2)}) collective-permute-start(f32[4,1,128]{2,1,0:T(1,128)S(1)} %mul.169), channel_id=1, source_target_pairs={{0,4},{2,6},{4,8},{6,10},{8,12},{10,14},{12,16},{14,18},{16,20},{1... | collective-permute-start | bytes 6152 | tf_op jit(solution)/shard_map/ppermute | solution.py:182
  107.5 25.4 %collective-permute-start.18 = (f32[4,1,128]{2,1,0:T(1,128)S(1)}, f32[4,1,128]{2,1,0:T(1,128)S(1)}, u32[]{:S(2)}, u32[]{:S(2)}) collective-permute-start(f32[4,1,128]{2,1,0:T(1,128)S(1)} %mul.192), channel_id=1, source_target_pairs={{8,0},{10,2},{12,4},{14,6},{16,8},{18,10},{20,12},{22,14},{24,16},... | collective-permute-start | bytes 6152 | tf_op jit(solution)/shard_map/ppermute | solution.py:182
  108.8 24.1 %collective-permute-start.8 = (f32[4,1,128]{2,1,0:T(1,128)S(1)}, f32[4,1,128]{2,1,0:T(1,128)S(1)}, u32[]{:S(2)}, u32[]{:S(2)}) collective-permute-start(f32[4,1,128]{2,1,0:T(1,128)S(1)} %mul.173), channel_id=1, source_target_pairs={{0,8},{2,10},{4,12},{6,14},{8,16},{10,18},{12,20},{14,22},{16,24},... | collective-permute-start | bytes 6152 | tf_op jit(solution)/shard_map/ppermute | solution.py:182
  120.9 19.8 %collective-permute-start.7 = (bf16[4,256,128]{2,1,0:T(8,128)(2,1)S(1)}, bf16[4,256,128]{2,1,0:T(8,128)(2,1)S(1)}, u32[]{:S(2)}, u32[]{:S(2)}) collective-permute-start(bf16[4,256,128]{2,1,0:T(8,128)(2,1)S(1)} %fusion.7), channel_id=1, source_target_pairs={{0,8},{2,10},{4,12},{6,14},{8,16},{10,18},{12,20},{14,22},{16,24},... | collective-permute-start | bytes 786440 | tf_op jit(solution)/shard_map/ppermute | solution.py:182
  131.0 26.5 %collective-permute-start.19 = (bf16[4,256,128]{2,1,0:T(8,128)(2,1)S(1)}, bf16[4,256,128]{2,1,0:T(8,128)(2,1)S(1)}, u32[]{:S(2)}, u32[]{:S(2)}) collective-permute-start(bf16[4,256,128]{2,1,0:T(8,128)(2,1)S(1)} %fusion.6), channel_id=1, source_target_pairs={{16,0},{18,2},{20,4},{22,6},{24,8},{26,10},{28,12},{30,14},{17,1},... | collective-permute-start | bytes 786440 | tf_op jit(solution)/shard_map/ppermute | solution.py:182
  140.9 17.6 %collective-permute-start.9 = (bf16[4,256,128]{2,1,0:T(8,128)(2,1)S(1)}, bf16[4,256,128]{2,1,0:T(8,128)(2,1)S(1)}, u32[]{:S(2)}, u32[]{:S(2)}) collective-permute-start(bf16[4,256,128]{2,1,0:T(8,128)(2,1)S(1)} %fusion.5), channel_id=1, source_target_pairs={{0,16},{2,18},{4,20},{6,22},{8,24},{10,26},{12,28},{14,30},{1,17},... | collective-permute-start | bytes 786440 | tf_op jit(solution)/shard_map/ppermute | solution.py:182
  173.1 8.4 %copy-start.1 = (bf16[2048]{0:T(1024)(128)(2,1)S(1)}, bf16[2048]{0:T(1024)(128)(2,1)}, u32[]{:S(2)}) copy-start(bf16[2048]{0:T(1024)(128)(2,1)} %param.26) | copy-start | bytes 12292
  179.3 41.8 %collective-permute-start.20 = (bf16[512,2048]{1,0:T(8,128)(2,1)}, bf16[512,2048]{1,0:T(8,128)(2,1)}, u32[]{:S(2)}, u32[]{:S(2)}) collective-permute-start(bf16[512,2048]{1,0:T(8,128)(2,1)} %convolution_convert_fusion), channel_id=1, source_target_pairs={{0,1},{1,0},{2,3},{3,2},{4,5},{5,4},{6,7},{7,6},{8,9},{9,8},{10,11... | collective-permute-start | bytes 6291464 | tf_op jit(solution)/shard_map/ppermute | solution.py:187
  227.8 2.0 copy-start
  230.2 40.7 %collective-permute-start.21 = (bf16[512,2048]{1,0:T(8,128)(2,1)S(1)}, bf16[512,2048]{1,0:T(8,128)(2,1)}, u32[]{:S(2)}, u32[]{:S(2)}) collective-permute-start(bf16[512,2048]{1,0:T(8,128)(2,1)S(1)} %multiply_convert_fusion.2), channel_id=1, source_target_pairs={{0,1},{1,0},{2,3},{3,2},{4,5},{5,4},{6,7},{7,6},{8,9},{9,8},{10,11... | collective-permute-start | bytes 6291464 | tf_op jit(solution)/shard_map/ppermute | solution.py:187
  349.9 48.1 %collective-permute-start.22 = (bf16[512,2048]{1,0:T(8,128)(2,1)}, bf16[512,2048]{1,0:T(8,128)(2,1)}, u32[]{:S(2)}, u32[]{:S(2)}) collective-permute-start(bf16[512,2048]{1,0:T(8,128)(2,1)} %convolution_convert_fusion.2), channel_id=1, source_target_pairs={{0,1},{1,0},{2,3},{3,2},{4,5},{5,4},{6,7},{7,6},{8,9},{9,8},{10,11... | collective-permute-start | bytes 6291464 | tf_op jit(solution)/shard_map/ppermute | solution.py:187
Sparse Core Ops, SparseCore 0:
  9.6 111.9 all-gather.3
  123.9 105.2 all-gather.5
  231.4 95.1 all-gather.7

commit v2 on v1

--- a/solution.py
+++ b/solution.py
@@ -254,14 +254,22 @@
     normed = row_norm(resid, feedforward_norm_gain)
     others = [rotate(normed, "tp", s) for s in range(1, n)]
 
-    def feed(x):
-        hidden = (jax.nn.silu(dot(x, gate_all)) * dot(x, up_all)).astype(BF)
-        return dot(hidden, down_all).astype(BF)
-
-    returned = [rotate(feed(x), "tp", -s) for s, x in enumerate(others, 1)]
-    mlp_out = feed(normed).astype(F32)
-    for piece in returned:
-        mlp_out = mlp_out + piece.astype(F32)
+    def hidden_of(x):
+        return (jax.nn.silu(dot(x, gate_all)) * dot(x, up_all)).astype(BF)
+
+    own, *others = lax.optimization_barrier((hidden_of(normed), *others))
+    parts = 2
+    returned = []
+    for s, x in enumerate(others, 1):
+        hidden = hidden_of(x)
+        cut = [
+            rotate(dot(h, down_all).astype(BF), "tp", -s)
+            for h in jnp.split(hidden, parts, axis=0)
+        ]
+        returned.append(cut)
+    mlp_out = lax.optimization_barrier(dot(own, down_all).astype(BF)).astype(F32)
+    for cut in returned:
+        mlp_out = mlp_out + jnp.concatenate(cut, axis=0).astype(F32)
     return (resid + mlp_out).astype(BF)
 
 

time: 430 us -> 392 us (0.912)
  waiting for transfers between devices: 183 us -> 155 us
  matrix products: 84.8 us -> 71.6 us
    ppermute x3 -> x4, waiting for transfers between devices: 114 us -> 90.1 us  [rotate(): return lax.ppermute(x, axis, [(i, (i + by) % n) for i in range(n)])]
    dot_general x6 -> x9, matrix products: 84.8 us -> 71.6 us  [dot(): return jnp.dot(a, b, preferred_element_type=F32)]
  transfers between devices with their start and end apart: 26 -> 27, of which waited for: 8 -> 9; matrix products, arithmetic and copies ran while one was open for 11% -> 19% of each run, Pallas kernels for 9% -> 10%
where the time goes in v2:
time: 392 us; the launch traced here: 391 us
  waiting for transfers between devices  155 us (40%)
  starting transfers between devices  92.6 us (24%)
  matrix products  71.6 us (18%)
  Pallas kernels  38.1 us (10%)
  between operations  17.4 us (4%)
  other arithmetic  9.71 us (2%)
  local copies, waits for them, and re-layouts  6.63 us (2%)
    ppermute x4, waiting for transfers between devices, rotate(): return lax.ppermute(x, axis, [(i, (i + by) % n) for i in range(n)])  90.1 us
    ppermute x20, starting transfers between devices, shift(): lax.ppermute(x, axis, [(i, i + by) for i in range(n) if 0 <= i + by < n])  86.8 us
    dot_general x9, matrix products, dot(): return jnp.dot(a, b, preferred_element_type=F32)  71.6 us
    all_gather x1, waiting for transfers between devices, per_device(): down_all = lax.all_gather(down_weight, 'sp', axis=1, tiled=True)  39.4 us
    pallas_call x1, Pallas kernels, local_attention(): pl.pallas_call(local_kernel, grid=(heads,), in_specs=[lanes(dk), lanes(dk...  24.5 us
    ppermute x20, waiting for transfers between devices, shift(): lax.ppermute(x, axis, [(i, i + by) for i in range(n) if 0 <= i + by < n])  23.2 us
    pallas_call x1, Pallas kernels, head_mix(): pl.pallas_call(mix_kernel, grid=(heads, 4), in_specs=[pl.BlockSpec((tile,...  13.6 us
  transfers between devices with their start and end apart: 27, of which 9 were waited for; matrix products, arithmetic and copies ran while one was open for 19% of the time, Pallas kernels for 10%

profile of v2, /device:TPU:0, one launch (start us, length us, event | category | flops | bytes accessed | tf_op | source)
XLA Modules:
  0.0 390.9 jit_solution(10218732472048445379)
XLA Ops:
  12.9 24.5 %local_attention.1 = (f32[1024,1024]{1,0:T(8,128)}, bf16[1024,1024]{1,0:T(8,128)(2,1)}, f32[4,256,128]{2,1,0:T(8,128)}, f32[4,256,128]{2,1,0:T(8,128)}, f32[4,1,128]{2,1,0:T(1,128)}) custom-call(bf16[1024,512]{1,0:T(8,128)(2,1)} %q_ref.1, bf16[1024,512]{1,0:T(8,128)(2,1)} %k_ref.1, bf16[1024,1024]{1,0:T(8,128)(2,1)} %v_ref.1, bf16[1024,512]{1,0:T(8,128)(2,1)} %g_ref.1, ...), custom_call_target="tpu_custom_call" | custom-call | flops 60000002048 | bytes 20000000 | tf_op jit(solution)/shard_map/local_attention/pallas_call | solution.py:112
  40.9 3.0 collective-permute-start
  46.4 7.5 %collective-permute-start.1 = (f32[1]{0:T(128)}, f32[1]{0:T(128)}, u32[]{:S(2)}, u32[]{:S(2)}) collective-permute-start(f32[1]{0:T(128)} %add.82), channel_id=1, source_target_pairs={{0,2},{2,4},{4,6},{6,8},{8,10},{10,12},{12,14},{14,16},{16,18},{18... | collective-permute-start | bytes 20 | tf_op jit(solution)/shard_map/ppermute | solution.py:182
  62.1 5.3 %collective-permute-start.3 = (bf16[4,256,128]{2,1,0:T(8,128)(2,1)S(1)}, bf16[4,256,128]{2,1,0:T(8,128)(2,1)S(1)}, u32[]{:S(2)}, u32[]{:S(2)}) collective-permute-start(bf16[4,256,128]{2,1,0:T(8,128)(2,1)S(1)} %collective-permute-done), channel_id=1, source_target_pairs={{0,2},{2,4},{4,6},{6,8},{8,10},{10,12},{12,14},{14,16},{16,18},{18... | collective-permute-start | bytes 786440 | tf_op jit(solution)/shard_map/ppermute | solution.py:182
  70.1 4.3 %collective-permute-start.2 = (f32[4,1,128]{2,1,0:T(1,128)S(1)}, f32[4,1,128]{2,1,0:T(1,128)S(1)}, u32[]{:S(2)}, u32[]{:S(2)}) collective-permute-start(f32[4,1,128]{2,1,0:T(1,128)S(1)} %get-tuple-element.22), channel_id=1, source_target_pairs={{0,2},{2,4},{4,6},{6,8},{8,10},{10,12},{12,14},{14,16},{16,18},{18... | collective-permute-start | bytes 6152 | tf_op jit(solution)/shard_map/ppermute | solution.py:182
  75.3 17.2 %collective-permute-start.5 = (bf16[4,256,128]{2,1,0:T(8,128)(2,1)S(1)}, bf16[4,256,128]{2,1,0:T(8,128)(2,1)S(1)}, u32[]{:S(2)}, u32[]{:S(2)}) collective-permute-start(bf16[4,256,128]{2,1,0:T(8,128)(2,1)S(1)} %fusion.4), channel_id=1, source_target_pairs={{0,4},{2,6},{4,8},{6,10},{8,12},{10,14},{12,16},{14,18},{16,20},{1... | collective-permute-start | bytes 786440 | tf_op jit(solution)/shard_map/ppermute | solution.py:182
  94.0 6.5 %collective-permute-start.4 = (f32[4,1,128]{2,1,0:T(1,128)S(1)}, f32[4,1,128]{2,1,0:T(1,128)S(1)}, u32[]{:S(2)}, u32[]{:S(2)}) collective-permute-start(f32[4,1,128]{2,1,0:T(1,128)S(1)} %collective-permute-done.2), channel_id=1, source_target_pairs={{0,2},{2,4},{4,6},{6,8},{8,10},{10,12},{12,14},{14,16},{16,18},{18... | collective-permute-start | bytes 6152 | tf_op jit(solution)/shard_map/ppermute | solution.py:182
  101.8 5.1 %collective-permute-start.6 = (f32[4,1,128]{2,1,0:T(1,128)S(1)}, f32[4,1,128]{2,1,0:T(1,128)S(1)}, u32[]{:S(2)}, u32[]{:S(2)}) collective-permute-start(f32[4,1,128]{2,1,0:T(1,128)S(1)} %mul.169), channel_id=1, source_target_pairs={{0,4},{2,6},{4,8},{6,10},{8,12},{10,14},{12,16},{14,18},{16,20},{1... | collective-permute-start | bytes 6152 | tf_op jit(solution)/shard_map/ppermute | solution.py:182
  108.8 11.8 %collective-permute-start.8 = (f32[4,1,128]{2,1,0:T(1,128)S(1)}, f32[4,1,128]{2,1,0:T(1,128)S(1)}, u32[]{:S(2)}, u32[]{:S(2)}) collective-permute-start(f32[4,1,128]{2,1,0:T(1,128)S(1)} %mul.173), channel_id=1, source_target_pairs={{0,8},{2,10},{4,12},{6,14},{8,16},{10,18},{12,20},{14,22},{16,24},... | collective-permute-start | bytes 6152 | tf_op jit(solution)/shard_map/ppermute | solution.py:182
  120.8 9.9 %collective-permute-start.7 = (bf16[4,256,128]{2,1,0:T(8,128)(2,1)S(1)}, bf16[4,256,128]{2,1,0:T(8,128)(2,1)S(1)}, u32[]{:S(2)}, u32[]{:S(2)}) collective-permute-start(bf16[4,256,128]{2,1,0:T(8,128)(2,1)S(1)} %fusion.8), channel_id=1, source_target_pairs={{0,8},{2,10},{4,12},{6,14},{8,16},{10,18},{12,20},{14,22},{16,24},... | collective-permute-start | bytes 786440 | tf_op jit(solution)/shard_map/ppermute | solution.py:182
  132.8 7.4 %collective-permute-done.7 = bf16[4,256,128]{2,1,0:T(8,128)(2,1)S(1)} collective-permute-done((bf16[4,256,128]{2,1,0:T(8,128)(2,1)S(1)}, bf16[4,256,128]{2,1,0:T(8,128)(2,1)S(1)}, u32[]{:S(2)}, u32[]{:S(2)}) %collective-permute-start.7) | collective-permute-done | bytes 262176 | tf_op jit(solution)/shard_map/ppermute | solution.py:182
  140.4 3.3 collective-permute-start.9
  143.7 13.2 %collective-permute-done.19 = bf16[4,256,128]{2,1,0:T(8,128)(2,1)S(1)} collective-permute-done((bf16[4,256,128]{2,1,0:T(8,128)(2,1)S(1)}, bf16[4,256,128]{2,1,0:T(8,128)(2,1)S(1)}, u32[]{:S(2)}, u32[]{:S(2)}) %collective-permute-start.19) | collective-permute-done | bytes 262176 | tf_op jit(solution)/shard_map/ppermute | solution.py:182
  158.9 13.6 %head_mix.1 = bf16[1024,1024]{1,0:T(8,128)(2,1)} custom-call(f32[1024,1024]{1,0:T(8,128)} %get-tuple-element.12.o_ref, bf16[1024,1024]{1,0:T(8,128)(2,1)} %get-tuple-element.13.qc_ref, bf16[4,256,128]{2,1,0:T(8,128)(2,1)} %add_convert_fusion.2.cf_ref, bf16[4,256,128]{2,1,0:T(8,128)(2,1)} %add_convert_fusion.1.cb_ref, f32[1024,1]{1,0:T(8,128)} %copy.18.doc_ref, ...), custom_call_target="tpu_custom_call" | custom-call | flops 5000000000 | bytes 12000000 | tf_op jit(solution)/shard_map/head_mix/pallas_call | solution.py:159
  172.5 6.2 %convolution_convert_fusion = bf16[512,2048]{1,0:T(8,128)(2,1)} fusion(bf16[1024,2048]{1,0:T(8,128)(2,1)} %param.25, bf16[1024,1024]{1,0:T(8,128)(2,1)} %head_mix.1, s32[]{:T(128)S(6)} %select_n.23), kind=kOutput, calls=%fused_computation.6 | convolution fusion | flops 2148532224 | bytes 7340036 | tf_op jit(solution)/shard_map/dot_general | solution.py:211
  178.7 1.8 collective-permute-start.20
  180.5 39.5 %collective-permute-done.20 = bf16[512,2048]{1,0:T(8,128)(2,1)S(1)} collective-permute-done((bf16[512,2048]{1,0:T(8,128)(2,1)}, bf16[512,2048]{1,0:T(8,128)(2,1)S(1)}, u32[]{:S(2)}, u32[]{:S(2)}) %collective-permute-start.20) | collective-permute-done | bytes 2097184 | tf_op jit(solution)/shard_map/ppermute | solution.py:187
  220.0 6.1 %multiply_reduce_fusion = (f32[512]{0:T(512)S(1)}, f32[512,2048]{1,0:T(8,128)S(1)}) fusion(bf16[512,2048]{1,0:T(8,128)(2,1)S(1)} %collective-permute-done.20, bf16[1024,2048]{1,0:T(8,128)(2,1)} %param.25, bf16[1024,1024]{1,0:T(8,128)(2,1)} %head_mix.1, s32[]{:T(128)S(6)} %select_n.21, bf16[1024,2048]{1,0:T(8,128)(2,1)} %param.15), kind=kOutput, calls=%fused_computation.4 | convolution fusion | flops 2155871744 | bytes 13634560 | tf_op jit(solution)/shard_map/dot_general | solution.py:211
  226.1 2.0 copy-done
  228.5 1.8 collective-permute-start.21
  230.3 11.1 %fusion.13 = f32[512,2816]{1,0:T(8,128)} fusion(bf16[512,2048]{1,0:T(8,128)(2,1)S(1)} %multiply_convert_fusion.2, bf16[2048,2816]{1,0:T(8,128)(2,1)} %all-gather.4.cloned.1.call-done), kind=kOutput, calls=%fused_computation.36 | convolution fusion | flops 5905580032 | bytes 19398656 | tf_op jit(solution)/shard_map/dot_general | solution.py:211
  241.4 12.9 %multiply_convert_fusion.1 = bf16[512,2816]{1,0:T(8,128)(2,1)} fusion(f32[512,2816]{1,0:T(8,128)} %fusion.13, bf16[512,2048]{1,0:T(8,128)(2,1)S(1)} %multiply_convert_fusion.2, bf16[2048,2816]{1,0:T(8,128)(2,1)} %all-gather.6.cloned.1.call-done), kind=kOutput, calls=%fused_computation.1 | convolution fusion | flops 5914230784 | bytes 22282240 | tf_op jit(solution)/shard_map/dot_general | solution.py:211
  254.3 14.7 %collective-permute-done.21 = bf16[512,2048]{1,0:T(8,128)(2,1)} collective-permute-done((bf16[512,2048]{1,0:T(8,128)(2,1)S(1)}, bf16[512,2048]{1,0:T(8,128)(2,1)}, u32[]{:S(2)}, u32[]{:S(2)}) %collective-permute-start.21) | collective-permute-done | bytes 2097184 | tf_op jit(solution)/shard_map/ppermute | solution.py:187
  269.0 9.2 %fusion.14 = f32[512,2816]{1,0:T(8,128)} fusion(bf16[512,2048]{1,0:T(8,128)(2,1)} %collective-permute-done.21, bf16[2048,2816]{1,0:T(8,128)(2,1)S(1)} %copy-done.4), kind=kOutput, calls=%fused_computation.37 | convolution fusion | flops 5905580032 | bytes 19398656 | tf_op jit(solution)/shard_map/dot_general | solution.py:211
  278.2 8.9 %multiply_convert_fusion = bf16[512,2816]{1,0:T(8,128)(2,1)S(1)} fusion(f32[512,2816]{1,0:T(8,128)} %fusion.14, bf16[512,2048]{1,0:T(8,128)(2,1)} %collective-permute-done.21, bf16[2048,2816]{1,0:T(8,128)(2,1)S(1)} %bitcast.50), kind=kOutput, calls=%fused_computation | convolution fusion | flops 5914230784 | bytes 22282240 | tf_op jit(solution)/shard_map/dot_general | solution.py:211
  287.1 39.4 %all-gather.8.cloned.1.call-done = bf16[2816,2048]{1,0:T(8,128)(2,1)} async-done(((bf16[2816,128]{1,0:T(8,128)(2,1)}), bf16[2816,2048]{1,0:T(8,128)(2,1)}) %all-gather.8.cloned.1.call-update) | async-done | bytes 11534352 | tf_op jit(solution)/shard_map/all_gather | solution.py:221
  326.5 7.6 %convolution_convert_fusion.4 = bf16[256,2048]{1,0:T(8,128)(2,1)S(1)} fusion(bf16[2816,2048]{1,0:T(8,128)(2,1)} %all-gather.8.cloned.1.call-done, bf16[512,2816]{1,0:T(8,128)(2,1)S(1)} %multiply_convert_fusion), kind=kOutput, calls=%fused_computation.10 | convolution fusion | flops 2953314304 | bytes 14024704 | tf_op jit(solution)/shard_map/dot_general | solution.py:211
  335.7 3.2 convolution_convert_fusion.3
  339.5 6.5 %convolution_convert_fusion.2 = bf16[512,2048]{1,0:T(8,128)(2,1)S(1)} fusion(bf16[512,2816]{1,0:T(8,128)(2,1)S(1)} %copy-done.6, bf16[2816,2048]{1,0:T(8,128)(2,1)S(1)} %copy-done.3), kind=kOutput, calls=%fused_computation.8 | convolution fusion | flops 5906628608 | bytes 16515072 | tf_op jit(solution)/shard_map/dot_general | solution.py:211
  346.0 14.2 %collective-permute-done.22 = bf16[256,2048]{1,0:T(8,128)(2,1)S(1)} collective-permute-done((bf16[256,2048]{1,0:T(8,128)(2,1)S(1)}, bf16[256,2048]{1,0:T(8,128)(2,1)S(1)}, u32[]{:S(2)}, u32[]{:S(2)}) %collective-permute-start.22) | collective-permute-done | bytes 1048608 | tf_op jit(solution)/shard_map/ppermute | solution.py:187
  360.2 21.8 %collective-permute-done.23 = bf16[256,2048]{1,0:T(8,128)(2,1)S(1)} collective-permute-done((bf16[256,2048]{1,0:T(8,128)(2,1)S(1)}, bf16[256,2048]{1,0:T(8,128)(2,1)S(1)}, u32[]{:S(2)}, u32[]{:S(2)}) %collective-permute-start.23) | collective-permute-done | bytes 1048608 | tf_op jit(solution)/shard_map/ppermute | solution.py:187
  382.0 2.4 add_convert_fusion
  (85 shorter events, 31.7 us)
Async XLA Ops:
  6.5 223.7 %all-gather.4.cloned.1.call-start = ((), (), s32[]{:S(2)}) async-start(), calls=%async_computation | async-start | bytes 12255232 | tf_op jit(solution)/shard_map/all_gather | solution.py:219
  7.3 234.1 %all-gather.6.cloned.1.call-start = ((), (), s32[]{:S(2)}) async-start(), calls=%async_computation.1 | async-start | bytes 12255232 | tf_op jit(solution)/shard_map/all_gather | solution.py:220
  8.0 318.5 %all-gather.8.cloned.1.call-start = ((), (), s32[]{:S(2)}) async-start(), calls=%async_computation.2 | async-start | bytes 12255232 | tf_op jit(solution)/shard_map/all_gather | solution.py:221
  37.4 69.5 %copy-start.5 = (bf16[256]{0:T(256)(128)(2,1)S(1)}, bf16[256]{0:T(256)(128)(2,1)}, u32[]{:S(2)}) copy-start(bf16[256]{0:T(256)(128)(2,1)} %param.24) | copy-start | bytes 1540
  38.5 5.4 %collective-permute-start.10 = (bf16[4,256,128]{2,1,0:T(8,128)(2,1)S(1)}, bf16[4,256,128]{2,1,0:T(8,128)(2,1)S(1)}, u32[]{:S(2)}, u32[]{:S(2)}) collective-permute-start(bf16[4,256,128]{2,1,0:T(8,128)(2,1)S(1)} %convert_element_type.126), channel_id=1, source_target_pairs={{2,0},{4,2},{6,4},{8,6},{10,8},{12,10},{14,12},{16,14},{18,16},{20... | collective-permute-start | bytes 786440 | tf_op jit(solution)/shard_map/ppermute | solution.py:182
  40.9 21.2 %collective-permute-start = (bf16[4,256,128]{2,1,0:T(8,128)(2,1)S(1)}, bf16[4,256,128]{2,1,0:T(8,128)(2,1)S(1)}, u32[]{:S(2)}, u32[]{:S(2)}) collective-permute-start(bf16[4,256,128]{2,1,0:T(8,128)(2,1)S(1)} %convert_element_type.116), channel_id=1, source_target_pairs={{0,2},{2,4},{4,6},{6,8},{8,10},{10,12},{12,14},{14,16},{16,18},{18... | collective-permute-start | bytes 786440 | tf_op jit(solution)/shard_map/ppermute | solution.py:182
  43.9 23.5 %collective-permute-start.13 = (bf16[4,256,128]{2,1,0:T(8,128)(2,1)S(1)}, bf16[4,256,128]{2,1,0:T(8,128)(2,1)S(1)}, u32[]{:S(2)}, u32[]{:S(2)}) collective-permute-start(bf16[4,256,128]{2,1,0:T(8,128)(2,1)S(1)} %collective-permute-done.10), channel_id=1, source_target_pairs={{2,0},{4,2},{6,4},{8,6},{10,8},{12,10},{14,12},{16,14},{18,16},{20... | collective-permute-start | bytes 786440 | tf_op jit(solution)/shard_map/ppermute | solution.py:182
  46.4 9.5 %collective-permute-start.1 = (f32[1]{0:T(128)}, f32[1]{0:T(128)}, u32[]{:S(2)}, u32[]{:S(2)}) collective-permute-start(f32[1]{0:T(128)} %add.82), channel_id=1, source_target_pairs={{0,2},{2,4},{4,6},{6,8},{8,10},{10,12},{12,14},{14,16},{16,18},{18... | collective-permute-start | bytes 20 | tf_op jit(solution)/shard_map/ppermute | solution.py:182
  54.6 4.2 %collective-permute-start.11 = (f32[1]{0:T(128)}, f32[1]{0:T(128)}, u32[]{:S(2)}, u32[]{:S(2)}) collective-permute-start(f32[1]{0:T(128)} %add.87), channel_id=1, source_target_pairs={{2,0},{4,2},{6,4},{8,6},{10,8},{12,10},{14,12},{16,14},{18,16},{20... | collective-permute-start | bytes 20 | tf_op jit(solution)/shard_map/ppermute | solution.py:182
  60.8 6.6 %collective-permute-start.12 = (f32[4,1,128]{2,1,0:T(1,128)S(1)}, f32[4,1,128]{2,1,0:T(1,128)S(1)}, u32[]{:S(2)}, u32[]{:S(2)}) collective-permute-start(f32[4,1,128]{2,1,0:T(1,128)S(1)} %get-tuple-element.21), channel_id=1, source_target_pairs={{2,0},{4,2},{6,4},{8,6},{10,8},{12,10},{14,12},{16,14},{18,16},{20... | collective-permute-start | bytes 6152 | tf_op jit(solution)/shard_map/ppermute | solution.py:182
  62.1 13.1 %collective-permute-start.3 = (bf16[4,256,128]{2,1,0:T(8,128)(2,1)S(1)}, bf16[4,256,128]{2,1,0:T(8,128)(2,1)S(1)}, u32[]{:S(2)}, u32[]{:S(2)}) collective-permute-start(bf16[4,256,128]{2,1,0:T(8,128)(2,1)S(1)} %collective-permute-done), channel_id=1, source_target_pairs={{0,2},{2,4},{4,6},{6,8},{8,10},{10,12},{12,14},{14,16},{16,18},{18... | collective-permute-start | bytes 786440 | tf_op jit(solution)/shard_map/ppermute | solution.py:182
  67.5 25.0 %collective-permute-start.15 = (bf16[4,256,128]{2,1,0:T(8,128)(2,1)S(1)}, bf16[4,256,128]{2,1,0:T(8,128)(2,1)S(1)}, u32[]{:S(2)}, u32[]{:S(2)}) collective-permute-start(bf16[4,256,128]{2,1,0:T(8,128)(2,1)S(1)} %fusion.5), channel_id=1, source_target_pairs={{4,0},{6,2},{8,4},{10,6},{12,8},{14,10},{16,12},{18,14},{20,16},{2... | collective-permute-start | bytes 786440 | tf_op jit(solution)/shard_map/ppermute | solution.py:182
  68.8 5.6 %collective-permute-start.14 = (f32[4,1,128]{2,1,0:T(1,128)S(1)}, f32[4,1,128]{2,1,0:T(1,128)S(1)}, u32[]{:S(2)}, u32[]{:S(2)}) collective-permute-start(f32[4,1,128]{2,1,0:T(1,128)S(1)} %collective-permute-done.12), channel_id=1, source_target_pairs={{2,0},{4,2},{6,4},{8,6},{10,8},{12,10},{14,12},{16,14},{18,16},{20... | collective-permute-start | bytes 6152 | tf_op jit(solution)/shard_map/ppermute | solution.py:182
  70.1 5.1 %collective-permute-start.2 = (f32[4,1,128]{2,1,0:T(1,128)S(1)}, f32[4,1,128]{2,1,0:T(1,128)S(1)}, u32[]{:S(2)}, u32[]{:S(2)}) collective-permute-start(f32[4,1,128]{2,1,0:T(1,128)S(1)} %get-tuple-element.22), channel_id=1, source_target_pairs={{0,2},{2,4},{4,6},{6,8},{8,10},{10,12},{12,14},{14,16},{16,18},{18... | collective-permute-start | bytes 6152 | tf_op jit(solution)/shard_map/ppermute | solution.py:182
  75.3 45.4 %collective-permute-start.5 = (bf16[4,256,128]{2,1,0:T(8,128)(2,1)S(1)}, bf16[4,256,128]{2,1,0:T(8,128)(2,1)S(1)}, u32[]{:S(2)}, u32[]{:S(2)}) collective-permute-start(bf16[4,256,128]{2,1,0:T(8,128)(2,1)S(1)} %fusion.4), channel_id=1, source_target_pairs={{0,4},{2,6},{4,8},{6,10},{8,12},{10,14},{12,16},{14,18},{16,20},{1... | collective-permute-start | bytes 786440 | tf_op jit(solution)/shard_map/ppermute | solution.py:182
  92.7 38.1 %collective-permute-start.17 = (bf16[4,256,128]{2,1,0:T(8,128)(2,1)S(1)}, bf16[4,256,128]{2,1,0:T(8,128)(2,1)S(1)}, u32[]{:S(2)}, u32[]{:S(2)}) collective-permute-start(bf16[4,256,128]{2,1,0:T(8,128)(2,1)S(1)} %fusion.9), channel_id=1, source_target_pairs={{8,0},{10,2},{12,4},{14,6},{16,8},{18,10},{20,12},{22,14},{24,16},... | collective-permute-start | bytes 786440 | tf_op jit(solution)/shard_map/ppermute | solution.py:182
  94.0 7.8 %collective-permute-start.4 = (f32[4,1,128]{2,1,0:T(1,128)S(1)}, f32[4,1,128]{2,1,0:T(1,128)S(1)}, u32[]{:S(2)}, u32[]{:S(2)}) collective-permute-start(f32[4,1,128]{2,1,0:T(1,128)S(1)} %collective-permute-done.2), channel_id=1, source_target_pairs={{0,2},{2,4},{4,6},{6,8},{8,10},{10,12},{12,14},{14,16},{16,18},{18... | collective-permute-start | bytes 6152 | tf_op jit(solution)/shard_map/ppermute | solution.py:182
  100.4 7.0 %collective-permute-start.16 = (f32[4,1,128]{2,1,0:T(1,128)S(1)}, f32[4,1,128]{2,1,0:T(1,128)S(1)}, u32[]{:S(2)}, u32[]{:S(2)}) collective-permute-start(f32[4,1,128]{2,1,0:T(1,128)S(1)} %mul.188), channel_id=1, source_target_pairs={{4,0},{6,2},{8,4},{10,6},{12,8},{14,10},{16,12},{18,14},{20,16},{2... | collective-permute-start | bytes 6152 | tf_op jit(solution)/shard_map/ppermute | solution.py:182
  101.8 7.0 %collective-permute-start.6 = (f32[4,1,128]{2,1,0:T(1,128)S(1)}, f32[4,1,128]{2,1,0:T(1,128)S(1)}, u32[]{:S(2)}, u32[]{:S(2)}) collective-permute-start(f32[4,1,128]{2,1,0:T(1,128)S(1)} %mul.169), channel_id=1, source_target_pairs={{0,4},{2,6},{4,8},{6,10},{8,12},{10,14},{12,16},{14,18},{16,20},{1... | collective-permute-start | bytes 6152 | tf_op jit(solution)/shard_map/ppermute | solution.py:182
  107.5 25.3 %collective-permute-start.18 = (f32[4,1,128]{2,1,0:T(1,128)S(1)}, f32[4,1,128]{2,1,0:T(1,128)S(1)}, u32[]{:S(2)}, u32[]{:S(2)}) collective-permute-start(f32[4,1,128]{2,1,0:T(1,128)S(1)} %mul.192), channel_id=1, source_target_pairs={{8,0},{10,2},{12,4},{14,6},{16,8},{18,10},{20,12},{22,14},{24,16},... | collective-permute-start | bytes 6152 | tf_op jit(solution)/shard_map/ppermute | solution.py:182
  108.8 24.0 %collective-permute-start.8 = (f32[4,1,128]{2,1,0:T(1,128)S(1)}, f32[4,1,128]{2,1,0:T(1,128)S(1)}, u32[]{:S(2)}, u32[]{:S(2)}) collective-permute-start(f32[4,1,128]{2,1,0:T(1,128)S(1)} %mul.173), channel_id=1, source_target_pairs={{0,8},{2,10},{4,12},{6,14},{8,16},{10,18},{12,20},{14,22},{16,24},... | collective-permute-start | bytes 6152 | tf_op jit(solution)/shard_map/ppermute | solution.py:182
  120.8 19.4 %collective-permute-start.7 = (bf16[4,256,128]{2,1,0:T(8,128)(2,1)S(1)}, bf16[4,256,128]{2,1,0:T(8,128)(2,1)S(1)}, u32[]{:S(2)}, u32[]{:S(2)}) collective-permute-start(bf16[4,256,128]{2,1,0:T(8,128)(2,1)S(1)} %fusion.8), channel_id=1, source_target_pairs={{0,8},{2,10},{4,12},{6,14},{8,16},{10,18},{12,20},{14,22},{16,24},... | collective-permute-start | bytes 786440 | tf_op jit(solution)/shard_map/ppermute | solution.py:182
  130.9 26.1 %collective-permute-start.19 = (bf16[4,256,128]{2,1,0:T(8,128)(2,1)S(1)}, bf16[4,256,128]{2,1,0:T(8,128)(2,1)S(1)}, u32[]{:S(2)}, u32[]{:S(2)}) collective-permute-start(bf16[4,256,128]{2,1,0:T(8,128)(2,1)S(1)} %fusion.7), channel_id=1, source_target_pairs={{16,0},{18,2},{20,4},{22,6},{24,8},{26,10},{28,12},{30,14},{17,1},... | collective-permute-start | bytes 786440 | tf_op jit(solution)/shard_map/ppermute | solution.py:182
  140.4 17.5 %collective-permute-start.9 = (bf16[4,256,128]{2,1,0:T(8,128)(2,1)S(1)}, bf16[4,256,128]{2,1,0:T(8,128)(2,1)S(1)}, u32[]{:S(2)}, u32[]{:S(2)}) collective-permute-start(bf16[4,256,128]{2,1,0:T(8,128)(2,1)S(1)} %fusion.6), channel_id=1, source_target_pairs={{0,16},{2,18},{4,20},{6,22},{8,24},{10,26},{12,28},{14,30},{1,17},... | collective-permute-start | bytes 786440 | tf_op jit(solution)/shard_map/ppermute | solution.py:182
  178.7 41.3 %collective-permute-start.20 = (bf16[512,2048]{1,0:T(8,128)(2,1)}, bf16[512,2048]{1,0:T(8,128)(2,1)S(1)}, u32[]{:S(2)}, u32[]{:S(2)}) collective-permute-start(bf16[512,2048]{1,0:T(8,128)(2,1)} %convolution_convert_fusion), channel_id=1, source_target_pairs={{0,1},{1,0},{2,3},{3,2},{4,5},{5,4},{6,7},{7,6},{8,9},{9,8},{10,11... | collective-permute-start | bytes 6291464 | tf_op jit(solution)/shard_map/ppermute | solution.py:187
  228.5 40.5 %collective-permute-start.21 = (bf16[512,2048]{1,0:T(8,128)(2,1)S(1)}, bf16[512,2048]{1,0:T(8,128)(2,1)}, u32[]{:S(2)}, u32[]{:S(2)}) collective-permute-start(bf16[512,2048]{1,0:T(8,128)(2,1)S(1)} %multiply_convert_fusion.2), channel_id=1, source_target_pairs={{0,1},{1,0},{2,3},{3,2},{4,5},{5,4},{6,7},{7,6},{8,9},{9,8},{10,11... | collective-permute-start | bytes 6291464 | tf_op jit(solution)/shard_map/ppermute | solution.py:187
  241.4 27.6 %copy-start.4 = (bf16[2048,2816]{1,0:T(8,128)(2,1)S(1)}, bf16[2048,2816]{1,0:T(8,128)(2,1)}, u32[]{:S(2)}) copy-start(bf16[2048,2816]{1,0:T(8,128)(2,1)} %all-gather.4.cloned.1.call-done) | copy-start | bytes 34603012
  241.4 36.8 %slice-start = ((s8[11534336]{0:T(1024)(128)(4,1)}), s8[4194304]{0:T(1024)(128)(4,1)S(1)}, s32[]{:S(2)}) async-start(s8[11534336]{0:T(1024)(128)(4,1)} %bitcast.49), calls=%async_computation.3 | async-start | bytes 8388608
  241.4 36.8 %slice-start.1 = ((s8[11534336]{0:T(1024)(128)(4,1)}), s8[4194304]{0:T(1024)(128)(4,1)S(1)}, s32[]{:S(2)}) async-start(s8[11534336]{0:T(1024)(128)(4,1)} %bitcast.49), calls=%async_computation.4 | async-start | bytes 8388608
  334.1 26.1 %collective-permute-start.22 = (bf16[256,2048]{1,0:T(8,128)(2,1)S(1)}, bf16[256,2048]{1,0:T(8,128)(2,1)S(1)}, u32[]{:S(2)}, u32[]{:S(2)}) collective-permute-start(bf16[256,2048]{1,0:T(8,128)(2,1)S(1)} %convolution_convert_fusion.4), channel_id=1, source_target_pairs={{0,1},{1,0},{2,3},{3,2},{4,5},{5,4},{6,7},{7,6},{8,9},{9,8},{10,11... | collective-permute-start | bytes 3145736 | tf_op jit(solution)/shard_map/ppermute | solution.py:187
  338.9 43.1 %copy-start.1 = (f32[512,2048]{1,0:T(8,128)S(1)}, f32[512,2048]{1,0:T(8,128)}, u32[]{:S(2)}) copy-start(f32[512,2048]{1,0:T(8,128)} %copy-done) | copy-start | bytes 12582916
  338.9 43.0 %collective-permute-start.23 = (bf16[256,2048]{1,0:T(8,128)(2,1)S(1)}, bf16[256,2048]{1,0:T(8,128)(2,1)S(1)}, u32[]{:S(2)}, u32[]{:S(2)}) collective-permute-start(bf16[256,2048]{1,0:T(8,128)(2,1)S(1)} %convolution_convert_fusion.3), channel_id=1, source_target_pairs={{0,1},{1,0},{2,3},{3,2},{4,5},{5,4},{6,7},{7,6},{8,9},{9,8},{10,11... | collective-permute-start | bytes 3145736 | tf_op jit(solution)/shard_map/ppermute | solution.py:187
  (5 other events, 48.4 us)
Sparse Core Ops, SparseCore 0:
  9.6 111.9 all-gather.3
  123.9 105.2 all-gather.5
  231.3 95.1 all-gather.7
